TPU v7x, 512 devices: a whole 4x8x8 slice. The times are simulated.
512 devices in a mesh: sp: 128 (over z, y, core), tp: 4 (over x).
Axes of the slice: x: 4, y: 8, z: 8, core: 2. Of those that a mesh axis runs over, the one named last changes fastest.
Arguments:
- tokens: bfloat16 [16384, 2048], P(('sp', 'tp')), may hold values from -6 to 6
- norm_gain: float32 [2048], replicated, may hold values from 0.1 to 1.9
- w_filter_b: bfloat16 [2048, 1024], P('sp', 'tp'), may hold values from -0.125 to 0.125
- w_filter_c: bfloat16 [2048, 1024], P('sp', 'tp'), may hold values from -0.125 to 0.125
- w_filter_v: bfloat16 [2048, 1024], P('sp', 'tp'), may hold values from -0.125 to 0.125
- filter_taps: float32 [3, 1024], P(None, 'tp'), may hold values from -3.5 to 3.5
- w_query: bfloat16 [2048, 1024], P('sp', 'tp'), may hold values from -0.125 to 0.125
- retention_gate_matrix: bfloat16 [2048, 1024], P('sp', 'tp'), may hold values from -0.125 to 0.125
- w_input: bfloat16 [2048, 1024], P('sp', 'tp'), may hold values from -0.125 to 0.125
- forget_gap: float32 [1024], P('tp'), may hold values from 0 to 0.12
- additive_fade_log: float32 [16384, 1024], P('sp', 'tp'), may hold values from -1.1 to 0
- head_gain: float32 [128], replicated, may hold values from 0.1 to 1.9
- initial_state: float32 [8, 128, 128], P('tp'), may hold values from -0.013671875 to 0.013671875
- w_out_filter: bfloat16 [1024, 2048], P('tp'), may hold values from -0.125 to 0.125
- w_out_rec: bfloat16 [1024, 2048], P('tp'), may hold values from -0.125 to 0.125
Outputs:
- mixed: bfloat16 [16384, 2048], P(('sp', 'tp'))
All inputs are finite; a program needn't handle non-finite values.
Results may differ from a plain program's by a relative error of at most 0.03.
Values may be sent and summed in bfloat16 or wider, within the bound.
No kernel may reach another device: no remote copies, remote signals or barrier semaphores. Data moves between devices by JAX's collectives and lax.ppermute only.
A program may use at most 64 MiB of HBM per device.

v0:
```python
import jax
import jax.numpy as jnp
from jax import lax
from jax.sharding import Mesh
from jax.sharding import PartitionSpec as P

HEAD_DIM = 128
SPAN = 64
TAPS = 3
SP = ("sp_0", "sp_1", "sp_2")
SP_TP = ("sp_0", "sp_1", "sp_2", "tp")


epsilon = 1e-06


def in_order(blocks, dim):
    blocks = jnp.moveaxis(blocks, 0, dim)
    lengths = blocks.shape
    return blocks.reshape(*lengths[:dim], lengths[dim] * lengths[dim + 1], *lengths[dim + 2 :])


def sent_to_all(x, axis):
    copies = jnp.broadcast_to(x, (lax.axis_size(axis), *x.shape))
    return lax.all_to_all(copies, axis, split_axis=0, concat_axis=0, tiled=True)


def gathered_copies(x, axis, dim):
    return in_order(sent_to_all(x, axis), dim)


def in_one_piece(arrays, axis, dim, along):
    widths = [a.shape[along] for a in arrays]
    both = jnp.concatenate(arrays, axis=along)
    filled = lax.all_gather(both, axis, axis=dim, tiled=True)
    return tuple(jnp.split(filled, [sum(widths[:k]) for k in range(1, len(widths))], axis=along))


def shifted(block, axis, distance):
    devices = range(lax.axis_size(axis))
    route = [(i - distance, i) for i in devices if i - distance in devices]
    return lax.ppermute(block, axis, route)


def neutral_like(x, identity):
    return jax.tree.map(
        lambda part, zero: jnp.zeros_like(part) + jnp.asarray(zero, part.dtype), x, identity
    )


def prefix_by_axis(x, axes, combine, identity):
    before = start = neutral_like(x, identity)
    so_far = x
    for axis in reversed(axes):
        size, position = (lax.axis_size(axis), lax.axis_index(axis))
        pieces = jax.tree.map(
            lambda part, kind: lax.all_gather(part.astype(kind), axis),
            so_far,
            (jnp.bfloat16, jnp.bfloat16),
        )
        inside, so_far = (start, start)
        for k in range(size):
            passed = k < position
            so_far = combine(
                so_far, jax.tree.map(lambda part, own: part[k].astype(own.dtype), pieces, x)
            )
            inside = jax.tree.map(lambda new, old: jnp.where(passed, new, old), so_far, inside)
        before = combine(inside, before)
    return before


def split_up(x, dim, size):
    before, after = (x.shape[:dim], x.shape[dim + 1 :])
    return jnp.moveaxis(x.reshape(*before, size, -1, *after), dim, 0)


def sum_at_owner(x, axis, dim):
    blocks = split_up(x, dim, lax.axis_size(axis))
    arrived = lax.all_to_all(blocks, axis, split_axis=0, concat_axis=0, tiled=True)
    return arrived.astype(jnp.float32).sum(axis=0)


def project(normed, weight):
    return jnp.dot(normed, weight, preferred_element_type=jnp.float32).astype(jnp.bfloat16)


def block_step(carried_state, inputs):
    block_query, block_key, block_value_rows, block_decay = inputs
    causal = jnp.tril(jnp.ones((SPAN, SPAN), dtype=bool))
    running = jnp.cumsum(block_decay, axis=0)
    scaled_query = block_query * jnp.exp(running)
    key_scaled = block_key * jnp.exp(-running)
    scores = jnp.einsum("thk,shk->hts", scaled_query, key_scaled)
    scores = jnp.where(causal[None], scores, 0.0)
    final_result = jnp.einsum("hts,shv->thv", scores, block_value_rows)
    final_result = final_result + jnp.einsum("oql,qlz->oqz", scaled_query, carried_state)
    final_state = running[-1]
    key_remainder = block_key * jnp.exp(final_state[None] - running)
    updated_state = jnp.exp(final_state)[:, :, None] * carried_state + jnp.einsum(
        "dri,drz->riz", key_remainder, block_value_rows
    )
    return (updated_state, final_result)


def local_recurrence(normed, weights, forget_gap, additive_fade_log):
    queries = project(normed, weights[0]).astype(jnp.float32)
    forget_logit = project(normed, weights[1]).astype(jnp.float32)
    input_value = project(normed, weights[2]).astype(jnp.float32)
    key_rate = forget_gap * jax.nn.sigmoid(-forget_logit)
    log_decay = jnp.log1p(-key_rate) + additive_fade_log
    value_in = jax.nn.silu(input_value)
    length = queries.shape[0]
    head_count = queries.shape[1] // HEAD_DIM

    def heads_blocks(flat_rows):
        return flat_rows.reshape(length // SPAN, SPAN, head_count, HEAD_DIM)

    start_state = jnp.zeros((head_count, HEAD_DIM, HEAD_DIM), jnp.float32)
    end_state, within_block = lax.scan(
        block_step,
        start_state,
        (
            heads_blocks(queries),
            heads_blocks(key_rate),
            heads_blocks(value_in),
            heads_blocks(log_decay),
        ),
    )
    running = jnp.cumsum(log_decay.reshape(length, head_count, HEAD_DIM), axis=0)
    scaled_query = queries.reshape(length, head_count, HEAD_DIM) * jnp.exp(running)
    return (
        within_block.reshape(length, head_count, HEAD_DIM),
        scaled_query,
        running[-1],
        end_state,
    )


def chain_combine(earlier, later):
    return (earlier[0] + later[0], jnp.exp(later[0])[:, :, None] * earlier[1] + later[1])


def body(
    tokens,
    norm_gain,
    w_filter_b,
    w_filter_c,
    w_filter_v,
    filter_taps,
    w_query,
    retention_gate_matrix,
    w_input,
    forget_gap,
    additive_fade_log,
    head_gain,
    initial_state,
    w_out_filter,
    w_out_rec,
):
    gathered = gathered_copies(tokens, "tp", 0)
    widened = gathered.astype(jnp.float32)
    normed = (
        widened
        * lax.rsqrt(jnp.mean(widened * widened, axis=-1, keepdims=True) + epsilon)
        * norm_gain
    ).astype(jnp.bfloat16)
    recur_cols = in_one_piece((w_query, retention_gate_matrix, w_input), SP, 0, 1)
    within_block, scaled_query, decay_total, end_state = local_recurrence(
        normed, recur_cols, forget_gap, additive_fade_log
    )
    filter_cols = in_one_piece((w_filter_b, w_filter_c, w_filter_v), SP, 0, 1)
    gate_out = project(normed, filter_cols[0])
    product = project(normed, filter_cols[1]).astype(jnp.float32) * project(
        normed, filter_cols[2]
    ).astype(jnp.float32)
    length = product.shape[0]
    last_rows = product[length - (TAPS - 1) :]
    before = shifted(last_rows, SP, 1)
    decay_before, state_before = prefix_by_axis(
        (decay_total, end_state),
        SP,
        chain_combine,
        (jnp.zeros_like(decay_total), jnp.zeros_like(end_state)),
    )
    incoming_state = jnp.exp(decay_before)[:, :, None] * initial_state + state_before
    unmixed_output = within_block + jnp.einsum("oql,qlz->oqz", scaled_query, incoming_state)
    rec_out = (
        (
            unmixed_output
            * lax.rsqrt(jnp.mean(unmixed_output * unmixed_output, axis=-1, keepdims=True) + epsilon)
            * head_gain
        )
        .astype(jnp.bfloat16)
        .reshape(length, -1)
    )
    padded = jnp.concatenate([before, product], axis=0)
    filtered = jnp.zeros_like(product)
    for offset in range(TAPS):
        filtered = filtered + filter_taps[offset] * padded[offset : offset + length]
    filter_out = (gate_out.astype(jnp.float32) * filtered).astype(jnp.bfloat16)
    summed = sum_at_owner(
        (
            jnp.dot(filter_out, w_out_filter, preferred_element_type=jnp.float32)
            + jnp.dot(rec_out, w_out_rec, preferred_element_type=jnp.float32)
        ).astype(jnp.bfloat16),
        "tp",
        0,
    )
    return summed.astype(jnp.bfloat16)


def solution(mesh):
    torus = Mesh(mesh.devices.reshape(8, 8, 2, mesh.shape["tp"]), ("sp_0", "sp_1", "sp_2", "tp"))
    placed = (
        P(SP_TP, None),
        P(),
        P(SP, "tp"),
        P(SP, "tp"),
        P(SP, "tp"),
        P(None, "tp"),
        P(SP, "tp"),
        P(SP, "tp"),
        P(SP, "tp"),
        P("tp"),
        P(SP, "tp"),
        P(),
        P("tp", None, None),
        P("tp", None),
        P("tp", None),
    )
    return jax.shard_map(
        body, mesh=torus, in_specs=placed, out_specs=P(SP_TP, None), check_vma=False
    )
```

profile of v0, /device:TPU:1, one launch (start us, length us, event | category | flops | bytes accessed | tf_op | source)
XLA Modules:
  0.0 224.2 jit_solution(9690042726582239488)
XLA Ops:
  6.5 1.4 pad_maximum_fusion.2
  8.0 1.8 broadcast_in_dim.26
  9.8 4.8 %all-to-all-start = ((bf16[4,32,2048]{2,1,0:T(8,128)(2,1)}), bf16[4,32,2048]{2,1,0:T(8,128)(2,1)S(1)}, u32[]{:S(2)}, u32[]{:S(2)}) async-start(bf16[4,32,2048]{2,1,0:T(8,128)(2,1)} %broadcast_in_dim.26), calls=%async_computation | async-start | bytes 1048576 | tf_op jit(solution)/shard_map/all_to_all | solution.py:25
  14.6 1.3 pad_maximum_fusion.1
  16.8 4.7 %all-to-all-done = bf16[4,32,2048]{2,1,0:T(8,128)(2,1)S(1)} async-done(((bf16[4,32,2048]{2,1,0:T(8,128)(2,1)}), bf16[4,32,2048]{2,1,0:T(8,128)(2,1)S(1)}, u32[]{:S(2)}, u32[]{:S(2)}) %all-to-all-start) | async-done | bytes 524320 | tf_op jit(solution)/shard_map/all_to_all | solution.py:25
  21.8 0.9 fusion.41
  22.7 77.3 %all-gather.6.cloned.1.call-done = bf16[2048,768]{1,0:T(8,128)(2,1)} async-done(((bf16[16,768]{1,0:T(8,128)(2,1)}), bf16[2048,768]{1,0:T(8,128)(2,1)}) %all-gather.6.cloned.1.call-update) | async-done | bytes 3145744 | tf_op jit(solution)/shard_map/all_gather | solution.py:35
  100.1 1.6 log-plus-one_add_fusion
  101.7 1.5 fusion.23
  103.3 1.6 divide_multiply_fusion
  105.3 1.8 while.13
  107.3 1.8 all_gather.34
  109.1 11.2 %all_gather.35 = bf16[8,2,128]{2,1,0:T(2,128)(2,1)S(1)} all-gather(bf16[1,2,128]{2,1,0:T(2,128)(2,1)S(1)} %get-tuple-element.138), channel_id=1, replica_groups=mesh['sp_0'=8,'sp_1'=8,'sp_2'=2,'tp'=4] {'sp_1'}, dimensions={0}, use_global_device_ids=true | all-gather | bytes 4608 | tf_op jit(solution)/shard_map/all_gather | solution.py:57
  120.4 11.7 %all_gather.36 = bf16[8,2,128]{2,1,0:T(2,128)(2,1)S(1)} all-gather(bf16[1,2,128]{2,1,0:T(2,128)(2,1)S(1)} %get-tuple-element.124), channel_id=1, replica_groups=mesh['sp_0'=8,'sp_1'=8,'sp_2'=2,'tp'=4] {'sp_0'}, dimensions={0}, use_global_device_ids=true | all-gather | bytes 4608 | tf_op jit(solution)/shard_map/all_gather | solution.py:57
  132.1 8.8 %all-gather = bf16[4,128,128]{2,1,0:T(8,128)(2,1)S(1)} all-gather(bf16[2,128,128]{2,1,0:T(8,128)(2,1)S(1)} %convert_element_type.535), channel_id=2, replica_groups=mesh['sp_0'=8,'sp_1'=8,'sp_2'=2,'tp'=4] {'sp_2'}, dimensions={0}, use_global_device_ids=true | all-gather | bytes 196608 | tf_op jit(solution)/shard_map/all_gather | solution.py:57
  141.1 19.7 %all_gather.39 = bf16[8,2,128,128]{3,2,1,0:T(8,128)(2,1)S(1)} all-gather(bf16[1,2,128,128]{3,2,1,0:T(8,128)(2,1)S(1)} %fusion.87), channel_id=1, replica_groups=mesh['sp_0'=8,'sp_1'=8,'sp_2'=2,'tp'=4] {'sp_1'}, dimensions={0}, use_global_device_ids=true | all-gather | bytes 589824 | tf_op jit(solution)/shard_map/all_gather | solution.py:57
  161.1 21.5 %all_gather.40 = bf16[8,2,128,128]{3,2,1,0:T(8,128)(2,1)S(1)} all-gather(bf16[1,2,128,128]{3,2,1,0:T(8,128)(2,1)S(1)} %fusion.121), channel_id=1, replica_groups=mesh['sp_0'=8,'sp_1'=8,'sp_2'=2,'tp'=4] {'sp_0'}, dimensions={0}, use_global_device_ids=true | all-gather | bytes 589824 | tf_op jit(solution)/shard_map/all_gather | solution.py:57
  182.7 1.5 multiply_reduce_fusion.1
  184.6 1.5 fusion.32
  186.1 1.5 fusion.31
  187.7 11.9 %collective-permute-start = (f32[2,256]{1,0:T(2,128)S(1)}, f32[2,256]{1,0:T(2,128)S(1)}, u32[]{:S(2)}, u32[]{:S(2)}) collective-permute-start(f32[2,256]{1,0:T(2,128)S(1)} %slice.180), channel_id=1, source_target_pairs={{0,4},{4,8},{8,12},{12,16},{16,20},{20,24},{24,28},{28,32},{32,36}... | collective-permute-start | bytes 6152 | tf_op jit(solution)/shard_map/ppermute | solution.py:42
  200.3 2.0 fusion.122
  202.3 1.6 fusion.21
  203.9 12.8 %all_to_all.10 = bf16[4,32,2048]{2,1,0:T(8,128)(2,1)S(1)} all-to-all(bf16[4,32,2048]{2,1,0:T(8,128)(2,1)S(1)} %bitcast.307), channel_id=1, replica_groups=mesh['sp_0'=8,'sp_1'=8,'sp_2'=2,'tp'=4] {'tp'}, dimensions={0} | all-to-all | bytes 1048576 | tf_op jit(solution)/shard_map/all_to_all | solution.py:79
  (61 shorter events, 5.9 us)
Async XLA Ops:
  6.5 193.8 %copy-start = (bf16[256,2048]{1,0:T(8,128)(2,1)S(1)}, bf16[256,2048]{1,0:T(8,128)(2,1)}, u32[]{:S(2)}) copy-start(bf16[256,2048]{1,0:T(8,128)(2,1)} %param.30) | copy-start | bytes 3145732
  6.5 93.5 %copy-start.4 = (f32[256]{0:T(256)S(1)}, f32[256]{0:T(256)}, u32[]{:S(2)}) copy-start(f32[256]{0:T(256)} %param.26) | copy-start | bytes 3076
  6.5 93.5 %copy-start.2 = (f32[128,256]{1,0:T(8,128)S(1)}, f32[128,256]{1,0:T(8,128)}, u32[]{:S(2)}) copy-start(f32[128,256]{1,0:T(8,128)} %param.27) | copy-start | bytes 393220
  6.5 93.5 %all-gather.6.cloned.1.call-start = ((), (), s32[]{:S(2)}) async-start(), calls=%async_computation.3 | async-start | bytes 3170304 | tf_op jit(solution)/shard_map/all_gather | solution.py:35
  9.8 11.8 %all-to-all-start = ((bf16[4,32,2048]{2,1,0:T(8,128)(2,1)}), bf16[4,32,2048]{2,1,0:T(8,128)(2,1)S(1)}, u32[]{:S(2)}, u32[]{:S(2)}) async-start(bf16[4,32,2048]{2,1,0:T(8,128)(2,1)} %broadcast_in_dim.26), calls=%async_computation | async-start | bytes 1048576 | tf_op jit(solution)/shard_map/all_to_all | solution.py:25
  14.6 170.0 %all-gather.4.cloned.1.call-start = ((), (), s32[]{:S(2)}) async-start(), calls=%async_computation.2 | async-start | bytes 3170304 | tf_op jit(solution)/shard_map/all_gather | solution.py:35
  105.3 77.4 %copy-start.3 = (f32[2,128,128]{2,1,0:T(8,128)S(1)}, f32[2,128,128]{2,1,0:T(8,128)}, u32[]{:S(2)}) copy-start(f32[2,128,128]{2,1,0:T(8,128)} %param.29) | copy-start | bytes 393220
  182.7 16.9 %copy-start.1 = (f32[128]{0:T(128)S(1)}, f32[128]{0:T(128)}, u32[]{:S(2)}) copy-start(f32[128]{0:T(128)} %param.28) | copy-start | bytes 1540
  187.7 12.6 %collective-permute-start = (f32[2,256]{1,0:T(2,128)S(1)}, f32[2,256]{1,0:T(2,128)S(1)}, u32[]{:S(2)}, u32[]{:S(2)}) collective-permute-start(f32[2,256]{1,0:T(2,128)S(1)} %slice.180), channel_id=1, source_target_pairs={{0,4},{4,8},{8,12},{12,16},{16,20},{20,24},{24,28},{28,32},{32,36}... | collective-permute-start | bytes 6152 | tf_op jit(solution)/shard_map/ppermute | solution.py:42
Sparse Core Ops, SparseCore 0:
  10.5 89.5 all-gather.5
  103.2 81.3 all-gather.3
where the time goes:
time: 226 us; the launch traced here: 224 us
  blocking collectives  87.5 us (39%)
  waiting for transfers between devices  83.1 us (37%)
  starting transfers between devices  16.7 us (7%)
  matrix products  14 us (6%)
  between operations  13.7 us (6%)
  other arithmetic  5.88 us (3%)
  local copies, waits for them, and re-layouts  3.25 us (1%)
    all_gather x2, waiting for transfers between devices, in_one_piece(): filled = lax.all_gather(both, axis, axis=dim, tiled=True)  77.7 us
    all_gather x6, blocking collectives, prefix_by_axis(): lax.all_gather(part.astype(kind), axis)  74.7 us
    all_to_all x1, blocking collectives, sum_at_owner(): lax.all_to_all(blocks, axis, split_axis=0, concat_axis=0, tiled=True)  12.8 us
    ppermute x1, starting transfers between devices, shifted(): return lax.ppermute(block, axis, route)  11.9 us
    dot_general x5, matrix products, project(): jnp.dot(normed, weight, preferred_element_type=jnp.float32)  7.77 us
    all_to_all x1, starting transfers between devices, sent_to_all(): return lax.all_to_all(copies, axis, split_axis=0, concat_axis=0, tiled=True)  4.83 us
    all_to_all x1, waiting for transfers between devices, sent_to_all(): return lax.all_to_all(copies, axis, split_axis=0, concat_axis=0, tiled=True)  4.71 us
  transfers between devices with their start and end apart: 4, of which 4 were waited for; matrix products, arithmetic and copies ran while one was open for 6% of the time, Pallas kernels for 0%

commit v1 on v0

v1 whole, which is shorter than its diff:
```python
import jax
import jax.numpy as jnp
import numpy as np
from jax import lax
from jax.sharding import Mesh
from jax.sharding import PartitionSpec as P

HEAD_DIM = 128
SPAN = 64
TAPS = 3
HALO = 16
SP = ("sp_0", "sp_1", "sp_2")
SP_TP = ("sp_0", "sp_1", "sp_2", "tp")

epsilon = 1e-06
f32 = jnp.float32
bf16 = jnp.bfloat16


def exchanged(blocks, axis):
    return lax.all_to_all(blocks, axis, split_axis=0, concat_axis=0, tiled=True)


def sent_to_all(x, axis):
    return exchanged(jnp.broadcast_to(x, (lax.axis_size(axis), *x.shape)), axis)


def swapped(x, axis):
    return lax.ppermute(x, axis, [(0, 1), (1, 0)])


def shifted(block, axis):
    size = lax.axis_size(axis)
    return lax.ppermute(block, axis, [(i, i + 1) for i in range(size - 1)])


def running_sum(x):
    causal = jnp.tril(jnp.ones((x.shape[0], x.shape[0]), f32))
    return jnp.dot(causal, x, precision=lax.Precision.HIGHEST)


def rates(forget_logit, forget_gap, fade):
    key_rate = forget_gap * jax.nn.sigmoid(-forget_logit.astype(f32))
    return key_rate, jnp.log1p(-key_rate) + fade


def silu(v):
    return jax.nn.silu(v.astype(f32))


def state_of(key_rate, log_decay, value_in):
    running = running_sum(log_decay)
    remainder = (key_rate * jnp.exp(running[-1:] - running)).astype(bf16)
    state = jnp.einsum("tv,tk->vk", value_in.astype(bf16), remainder, preferred_element_type=f32)
    return running[-1], state


def pack(decay, state):
    high = lax.reduce_precision(decay, 8, 7)
    rest = decay - high
    low = lax.reduce_precision(rest, 8, 7)
    rows = jnp.stack([high, low, rest - low]).astype(bf16)
    return jnp.concatenate([state.astype(bf16), rows, jnp.zeros((13, HEAD_DIM), bf16)], axis=0)


def unpack(packed):
    decays = packed[:, HEAD_DIM : HEAD_DIM + 3].astype(f32).sum(axis=1)
    return decays, packed[:, :HEAD_DIM]


def weights_before(decays, position):
    size = decays.shape[0]
    place = jnp.arange(size)
    earlier = place < position
    kept = jnp.where(earlier[:, None], decays, 0.0)
    after = (place[None, :] > place[:, None]).astype(f32)
    since = jnp.sum(after[:, :, None] * kept[None], axis=1)
    return jnp.where(earlier[:, None], jnp.exp(since), 0.0), kept.sum(axis=0)


def weighted(weights, states):
    return jnp.sum(weights[:, None, :] * states.astype(f32), axis=0)


def body(
    tokens,
    norm_gain,
    w_filter_b,
    w_filter_c,
    w_filter_v,
    filter_taps,
    w_query,
    retention_gate_matrix,
    w_input,
    forget_gap,
    additive_fade_log,
    head_gain,
    initial_state,
    w_out_filter,
    w_out_rec,
):
    z, y, c = (lax.axis_index(a) for a in SP)
    own_rows = jnp.concatenate(
        [retention_gate_matrix, w_input, w_query, w_filter_b, w_filter_c, w_filter_v], axis=1
    )
    along_y = sent_to_all(own_rows, "sp_1").reshape(-1, own_rows.shape[1])
    weights = lax.all_gather(along_y, ("sp_0", "sp_2"), axis=0, tiled=True)

    gathered = sent_to_all(tokens, "tp").reshape(-1, tokens.shape[1])
    widened = gathered.astype(f32)
    normed = (
        widened
        * lax.rsqrt(jnp.mean(widened * widened, axis=-1, keepdims=True) + epsilon)
        * norm_gain
    ).astype(bf16)
    length, width = normed.shape
    order = np.arange(256).reshape(8, 2, 16).transpose(1, 0, 2).reshape(-1)
    swap = np.zeros((256, 256), np.float32)
    swap[order, np.arange(256)] = 1.0
    own = jnp.einsum(
        "tzk,kl->tzl",
        normed.reshape(length, 8, 256),
        jnp.asarray(swap, bf16),
        preferred_element_type=f32,
    ).astype(bf16).reshape(length, width)
    partner = swapped(own, "sp_2")
    halo = shifted(own[length - HALO :], SP)

    fade = additive_fade_log
    head = lambda a, k: lax.dynamic_slice_in_dim(a, k * HEAD_DIM, HEAD_DIM, axis=1)
    partner_fade = swapped(head(fade, 1 - c), "sp_2")

    chip = jnp.concatenate([own, partner], axis=0)
    chip_gates = jnp.dot(chip, weights[:, :512], preferred_element_type=f32).astype(bf16)
    forget_logit, input_value = chip_gates[:, :256], chip_gates[:, 256:]
    key_rate, log_decay = rates(forget_logit[:length], forget_gap, fade)
    value_in = silu(input_value[:length])
    gap_c = lax.dynamic_slice_in_dim(forget_gap, c * HEAD_DIM, HEAD_DIM)
    partner_rate, partner_decay = rates(head(forget_logit[length:], c), gap_c, partner_fade)
    partner_value = silu(head(input_value[length:], c))
    decay_own, state_own = state_of(head(key_rate, c), head(log_decay, c), head(value_in, c))
    decay_partner, state_partner = state_of(partner_rate, partner_decay, partner_value)
    first = c == 0
    decay_0, decay_1 = (
        jnp.where(first, decay_own, decay_partner),
        jnp.where(first, decay_partner, decay_own),
    )
    state_0, state_1 = (
        jnp.where(first, state_own, state_partner),
        jnp.where(first, state_partner, state_own),
    )
    state_chip = jnp.exp(decay_1)[None, :] * state_0 + state_1

    decays_y, states_y = unpack(sent_to_all(pack(decay_0 + decay_1, state_chip), "sp_1"))
    weights_row, decay_row = weights_before(decays_y, 8)
    row = weighted(weights_row, states_y)
    decays_z, states_z = unpack(sent_to_all(pack(decay_row, row), "sp_0"))
    weights_y, decay_y = weights_before(decays_y, y)
    inside = weighted(weights_y, states_y)
    weights_z, decay_z = weights_before(decays_z, z)
    start = lax.dynamic_index_in_dim(initial_state, c, keepdims=False).T
    before = jnp.exp(decay_z)[None, :] * start + weighted(weights_z, states_z)
    into_chip = jnp.exp(decay_y)[None, :] * before + inside
    into_second = jnp.exp(decay_0)[None, :] * into_chip + state_0
    incoming = exchanged(jnp.stack([into_chip, into_second]).astype(bf16), "sp_2")

    rest = jnp.dot(
        jnp.concatenate([halo, own], axis=0), weights[:, 512:], preferred_element_type=f32
    ).astype(bf16)
    queries = rest[HALO:, :256].astype(f32)
    gate_out = rest[HALO:, 256:512].astype(f32)
    product = rest[:, 512:768].astype(f32) * rest[:, 768:].astype(f32)
    filtered = jnp.zeros_like(gate_out)
    for offset in range(TAPS):
        at = HALO - (TAPS - 1) + offset
        filtered = filtered + filter_taps[offset] * product[at : at + length]
    filter_out = (gate_out * filtered).astype(bf16)
    filter_part = jnp.dot(filter_out, w_out_filter, preferred_element_type=f32)

    heads = lambda a: a.reshape(length // SPAN, SPAN, 2, HEAD_DIM)
    running = running_sum(log_decay)
    at_start = jnp.concatenate([jnp.zeros((1, 256), f32), running[SPAN - 1 : length - 1 : SPAN]])
    at_end = running[SPAN - 1 :: SPAN]
    within = running.reshape(length // SPAN, SPAN, 256) - at_start[:, None]
    scaled_query = heads((queries.reshape(within.shape) * jnp.exp(within)).astype(bf16))
    scaled_key = heads((key_rate.reshape(within.shape) * jnp.exp(-within)).astype(bf16))
    remainder = heads(
        (
            key_rate.reshape(within.shape)
            * jnp.exp(at_end[:, None] - running.reshape(within.shape))
        ).astype(bf16)
    )
    values = heads(value_in.astype(bf16))
    causal = jnp.tril(jnp.ones((SPAN, SPAN), dtype=bool))
    scores = jnp.einsum("bthk,bshk->bhts", scaled_query, scaled_key, preferred_element_type=f32)
    scores = jnp.where(causal, scores, 0.0).astype(bf16)
    local = jnp.einsum("bhts,bshv->bthv", scores, values, preferred_element_type=f32)
    cross = jnp.einsum("thk,shk->hts", scaled_query[1], remainder[0], preferred_element_type=f32)
    cross = jnp.einsum("hts,shv->thv", cross.astype(bf16), values[0], preferred_element_type=f32)
    local = jnp.concatenate([local[0], local[1] + cross], axis=0)
    full_query = (queries * jnp.exp(running)).astype(bf16).reshape(length, 2, HEAD_DIM)
    raw = local + jnp.einsum("thk,hvk->thv", full_query, incoming, preferred_element_type=f32)
    rec_out = (
        (raw * lax.rsqrt(jnp.mean(raw * raw, axis=-1, keepdims=True) + epsilon) * head_gain)
        .astype(bf16)
        .reshape(length, -1)
    )
    partial = (filter_part + jnp.dot(rec_out, w_out_rec, preferred_element_type=f32)).astype(bf16)
    arrived = exchanged(partial.reshape(4, length // 4, -1), "tp")
    return arrived.astype(f32).sum(axis=0).astype(bf16)


def solution(mesh):
    torus = Mesh(mesh.devices.reshape(8, 8, 2, mesh.shape["tp"]), ("sp_0", "sp_1", "sp_2", "tp"))
    placed = (
        P(SP_TP, None),
        P(),
        P(SP, "tp"),
        P(SP, "tp"),
        P(SP, "tp"),
        P(None, "tp"),
        P(SP, "tp"),
        P(SP, "tp"),
        P(SP, "tp"),
        P("tp"),
        P(SP, "tp"),
        P(),
        P("tp", None, None),
        P("tp", None),
        P("tp", None),
    )
    return jax.shard_map(
        body, mesh=torus, in_specs=placed, out_specs=P(SP_TP, None), check_vma=False
    )
```

time: 226 us -> 159 us (0.70)
  blocking collectives: 87.5 us -> 37 us
  waiting for transfers between devices: 83.1 us -> 53.3 us
  starting transfers between devices: 16.7 us -> 27.8 us
  local copies, waits for them, and re-layouts: 3.25 us -> 10.7 us
  matrix products: 14 us -> 8.98 us
    all_gather x6 -> x0, blocking collectives: 74.7 us -> none  [prefix_by_axis(): lax.all_gather(part.astype(kind), axis)]
    all_gather x2 -> x1, waiting for transfers between devices: 77.7 us -> 28 us  [body(): weights = lax.all_gather(along_y, ('sp_0', 'sp_2'), axis=0, tiled=True)]
    all_to_all x1 -> x3, blocking collectives: 12.8 us -> 37 us  [exchanged(): return lax.all_to_all(blocks, axis, split_axis=0, concat_axis=0, tiled=True)]
    all_to_all x1 -> x3, waiting for transfers between devices: 4.71 us -> 24 us  [exchanged(): return lax.all_to_all(blocks, axis, split_axis=0, concat_axis=0, tiled=True)]
    all_to_all x1 -> x3, starting transfers between devices: 4.83 us -> 15.8 us  [exchanged(): return lax.all_to_all(blocks, axis, split_axis=0, concat_axis=0, tiled=True)]
    dot_general x14 -> x13, matrix products: 14 us -> 8.98 us  [the longest x1 2.62 us: body(): jnp.dot(chip, weights[:, :512], preferred_element_type=f32).astype(bf16)]
    unnamed x10 -> x27, local copies, waits for them, and re-layouts: 0.02 us -> 4.51 us
    concatenate x2 -> x0, other arithmetic: 2.77 us -> none  [in_one_piece(): both = jnp.concatenate(arrays, axis=along)]
  transfers between devices with their start and end apart: 4 -> 7, of which waited for: 4 -> 5; matrix products, arithmetic and copies ran while one was open for 6% -> 7% of each run, Pallas kernels for 0% -> 0%
where the time goes in v1:
time: 159 us; the launch traced here: 158 us
  waiting for transfers between devices  53.3 us (34%)
  blocking collectives  37 us (23%)
  starting transfers between devices  27.8 us (17%)
  between operations  13.9 us (9%)
  local copies, waits for them, and re-layouts  10.7 us (7%)
  matrix products  8.98 us (6%)
  other arithmetic  5.94 us (4%)
    all_to_all x3, blocking collectives, exchanged(): return lax.all_to_all(blocks, axis, split_axis=0, concat_axis=0, tiled=True)  37 us
    all_gather x1, waiting for transfers between devices, body(): weights = lax.all_gather(along_y, ('sp_0', 'sp_2'), axis=0, tiled=True)  28 us
    all_to_all x3, waiting for transfers between devices, exchanged(): return lax.all_to_all(blocks, axis, split_axis=0, concat_axis=0, tiled=True)  24 us
    all_to_all x3, starting transfers between devices, exchanged(): return lax.all_to_all(blocks, axis, split_axis=0, concat_axis=0, tiled=True)  15.8 us
    ppermute x2, starting transfers between devices, swapped(): return lax.ppermute(x, axis, [(0, 1), (1, 0)])  9.76 us
    unnamed x27, local copies, waits for them, and re-layouts  4.51 us
    broadcast_in_dim x4, local copies, waits for them, and re-layouts, sent_to_all(): return exchanged(jnp.broadcast_to(x, (lax.axis_size(axis), *x.shape)), axis)  3.29 us
  transfers between devices with their start and end apart: 7, of which 5 were waited for; matrix products, arithmetic and copies ran while one was open for 7% of the time, Pallas kernels for 0%

profile of v1, /device:TPU:1, one launch (start us, length us, event | category | flops | bytes accessed | tf_op | source)
XLA Modules:
  0.0 157.7 jit_solution(3976584171746836471)
XLA Ops:
  6.6 0.8 constant_dynamic-update-slice_fusion.5
  10.9 19.2 %all_to_all.30 = bf16[8,16,1536]{2,1,0:T(8,128)(2,1)} all-to-all(bf16[8,16,1536]{2,1,0:T(8,128)(2,1)S(1)} %broadcast_in_dim.102), channel_id=1, replica_groups=mesh['sp_0'=8,'sp_1'=8,'sp_2'=2,'tp'=4] {'sp_1'}, dimensions={0} | all-to-all | bytes 786432 | tf_op jit(solution)/shard_map/all_to_all | solution.py:21
  30.1 1.8 %broadcast_in_dim.101 = bf16[4,32,2048]{2,1,0:T(8,128)(2,1)} broadcast(bf16[32,2048]{1,0:T(8,128)(2,1)} %param.16), dimensions={1,2} | broadcast | bytes 655360 | tf_op jit(solution)/shard_map/broadcast_in_dim | solution.py:25
  31.9 6.0 %all-to-all-start = ((bf16[4,32,2048]{2,1,0:T(8,128)(2,1)}), bf16[4,32,2048]{2,1,0:T(8,128)(2,1)S(1)}, u32[]{:S(2)}, u32[]{:S(2)}) async-start(bf16[4,32,2048]{2,1,0:T(8,128)(2,1)} %broadcast_in_dim.101), calls=%async_computation | async-start | bytes 1048576 | tf_op jit(solution)/shard_map/all_to_all | solution.py:21
  37.8 4.4 %collective-permute-start.2 = (f32[128,128]{1,0:T(8,128)S(1)}, f32[128,128]{1,0:T(8,128)S(1)}, u32[]{:S(2)}, u32[]{:S(2)}) collective-permute-start(f32[128,128]{1,0:T(8,128)S(1)} %constant_dynamic-slice_fusion.1), channel_id=1, source_target_pairs={{0,4},{4,0},{1,5},{5,1},{2,6},{6,2},{3,7},{7,3},{8,12},{12,8},{9,1... | collective-permute-start | bytes 196616 | tf_op jit(solution)/shard_map/ppermute | solution.py:29
  42.5 2.3 %all-to-all-done = bf16[4,32,2048]{2,1,0:T(8,128)(2,1)S(1)} async-done(((bf16[4,32,2048]{2,1,0:T(8,128)(2,1)}), bf16[4,32,2048]{2,1,0:T(8,128)(2,1)S(1)}, u32[]{:S(2)}, u32[]{:S(2)}) %all-to-all-start) | async-done | bytes 524320 | tf_op jit(solution)/shard_map/all_to_all | solution.py:21
  46.0 5.4 %collective-permute-start.1 = (bf16[128,2048]{0,1:T(8,128)(2,1)S(1)}, bf16[128,2048]{0,1:T(8,128)(2,1)}, u32[]{:S(2)}, u32[]{:S(2)}) collective-permute-start(bf16[128,2048]{0,1:T(8,128)(2,1)S(1)} %bitcast.98), channel_id=1, source_target_pairs={{0,4},{4,0},{1,5},{5,1},{2,6},{6,2},{3,7},{7,3},{8,12},{12,8},{9,1... | collective-permute-start | bytes 1572872 | tf_op jit(solution)/shard_map/ppermute | solution.py:29
  51.5 2.2 %collective-permute-start = (bf16[16,2048]{1,0:T(8,128)(2,1)S(1)}, bf16[16,2048]{1,0:T(8,128)(2,1)S(1)}, u32[]{:S(2)}, u32[]{:S(2)}) collective-permute-start(bf16[16,2048]{1,0:T(8,128)(2,1)S(1)} %bitcast.102), channel_id=1, source_target_pairs={{0,4},{4,8},{8,12},{12,16},{16,20},{20,24},{24,28},{28,32},{32,36}... | collective-permute-start | bytes 196616 | tf_op jit(solution)/shard_map/ppermute | solution.py:34
  53.6 1.3 collective-permute-done
  55.2 28.0 %all-gather.2.cloned.1.call-done = bf16[2048,1536]{1,0:T(8,128)(2,1)} async-done(((bf16[128,1536]{1,0:T(8,128)(2,1)}), bf16[2048,1536]{1,0:T(8,128)(2,1)}) %all-gather.2.cloned.1.call-update) | async-done | bytes 6291472 | tf_op jit(solution)/shard_map/all_gather | solution.py:107
  83.3 2.6 %fusion.8 = bf16[256,512]{1,0:T(8,128)(2,1)S(1)} fusion(bf16[2048,1536]{1,0:T(8,128)(2,1)} %all-gather.2.cloned.1.call-done, bf16[128,2048]{0,1:T(8,128)(2,1)} %collective-permute-done.1, bf16[128,2048]{0,1:T(8,128)(2,1)S(1)} %bitcast.99), kind=kOutput, calls=%fused_computation.8 | convolution fusion | flops 539099136 | bytes 3407872 | tf_op jit(solution)/shard_map/dot_general | solution.py:134
  86.1 0.8 copy-done.9
  86.9 1.3 fusion.5
  89.8 0.8 add_convert_fusion.1
  91.5 6.0 %all-to-all-start.2 = ((bf16[8,144,128]{2,1,0:T(8,128)(2,1)}), bf16[8,144,128]{2,1,0:T(8,128)(2,1)S(1)}, u32[]{:S(2)}, u32[]{:S(2)}) async-start(bf16[8,144,128]{2,1,0:T(8,128)(2,1)} %broadcast_in_dim.107), calls=%async_computation.2 | async-start | bytes 589824 | tf_op jit(solution)/shard_map/all_to_all | solution.py:21
  98.2 12.3 %all-to-all-done.2 = bf16[8,144,128]{2,1,0:T(8,128)(2,1)S(1)} async-done(((bf16[8,144,128]{2,1,0:T(8,128)(2,1)}), bf16[8,144,128]{2,1,0:T(8,128)(2,1)S(1)}, u32[]{:S(2)}, u32[]{:S(2)}) %all-to-all-start.2) | async-done | bytes 294944 | tf_op jit(solution)/shard_map/all_to_all | solution.py:21
  112.4 3.9 %all-to-all-start.3 = ((bf16[8,144,128]{2,1,0:T(8,128)(2,1)}), bf16[8,144,128]{2,1,0:T(8,128)(2,1)S(1)}, u32[]{:S(2)}, u32[]{:S(2)}) async-start(bf16[8,144,128]{2,1,0:T(8,128)(2,1)} %broadcast_in_dim.111), calls=%async_computation.3 | async-start | bytes 589824 | tf_op jit(solution)/shard_map/all_to_all | solution.py:21
  116.9 0.9 fusion.13
  118.1 9.4 %all-to-all-done.3 = bf16[8,144,128]{2,1,0:T(8,128)(2,1)S(1)} async-done(((bf16[8,144,128]{2,1,0:T(8,128)(2,1)}), bf16[8,144,128]{2,1,0:T(8,128)(2,1)S(1)}, u32[]{:S(2)}, u32[]{:S(2)}) %all-to-all-start.3) | async-done | bytes 294944 | tf_op jit(solution)/shard_map/all_to_all | solution.py:21
  127.9 0.9 convert_bitcast_fusion
  128.9 0.9 fusion.75
  129.8 5.5 %all_to_all.31 = bf16[2,128,128]{2,1,0:T(8,128)(2,1)S(1)} all-to-all(bf16[2,128,128]{2,1,0:T(8,128)(2,1)S(1)} %pad_maximum_fusion), channel_id=1, replica_groups=mesh['sp_0'=8,'sp_1'=8,'sp_2'=2,'tp'=4] {'sp_2'}, dimensions={0} | all-to-all | bytes 131072 | tf_op jit(solution)/shard_map/all_to_all | solution.py:21
  135.2 1.2 multiply_reduce_fusion.2
  137.7 12.4 %all_to_all.32 = bf16[4,32,2048]{2,1,0:T(8,128)(2,1)S(1)} all-to-all(bf16[4,32,2048]{2,1,0:T(8,128)(2,1)S(1)} %bitcast.94), channel_id=1, replica_groups=mesh['sp_0'=8,'sp_1'=8,'sp_2'=2,'tp'=4] {'tp'}, dimensions={0} | all-to-all | bytes 1048576 | tf_op jit(solution)/shard_map/all_to_all | solution.py:21
  (103 shorter events, 13.8 us)
Async XLA Ops:
  6.5 111.3 %copy-start = (bf16[256,2048]{1,0:T(8,128)(2,1)S(1)}, bf16[256,2048]{1,0:T(8,128)(2,1)}, u32[]{:S(2)}) copy-start(bf16[256,2048]{1,0:T(8,128)(2,1)} %param.29) | copy-start | bytes 3145732
  6.5 31.3 %copy-start.3 = (f32[128,256]{1,0:T(8,128)S(1)}, f32[128,256]{1,0:T(8,128)}, u32[]{:S(2)}) copy-start(f32[128,256]{1,0:T(8,128)} %param.26) | copy-start | bytes 393220
  6.5 35.7 %copy-start.5 = (f32[2,128,128]{2,1,0:T(8,128)S(1)}, f32[2,128,128]{2,1,0:T(8,128)}, u32[]{:S(2)}) copy-start(f32[2,128,128]{2,1,0:T(8,128)} %param.28) | copy-start | bytes 393220
  6.5 35.7 %copy-start.6 = (f32[2048]{0:T(1024)S(1)}, f32[2048]{0:T(1024)}, u32[]{:S(2)}) copy-start(f32[2048]{0:T(1024)} %param.17) | copy-start | bytes 24580
  6.5 35.9 %copy-start.8 = (f32[256]{0:T(256)S(1)}, f32[256]{0:T(256)}, u32[]{:S(2)}) copy-start(f32[256]{0:T(256)} %param.25) | copy-start | bytes 3076
  6.5 76.7 %all-gather.2.cloned.1.call-start = ((), (), s32[]{:S(2)}) async-start(), calls=%async_computation.6 | async-start | bytes 6684672 | tf_op jit(solution)/shard_map/all_gather | solution.py:107
  31.9 12.9 %all-to-all-start = ((bf16[4,32,2048]{2,1,0:T(8,128)(2,1)}), bf16[4,32,2048]{2,1,0:T(8,128)(2,1)S(1)}, u32[]{:S(2)}, u32[]{:S(2)}) async-start(bf16[4,32,2048]{2,1,0:T(8,128)(2,1)} %broadcast_in_dim.101), calls=%async_computation | async-start | bytes 1048576 | tf_op jit(solution)/shard_map/all_to_all | solution.py:21
  37.8 7.6 %copy-start.4 = (bf16[256,256,1]{1,0,2:T(8,128)(2,1)S(1)}, bf16[256,256,1]{1,0,2:T(8,128)(2,1)}, u32[]{:S(2)}) copy-start(bf16[256,256,1]{1,0,2:T(8,128)(2,1)} %constant.72) | copy-start | bytes 393220
  37.8 50.8 %collective-permute-start.2 = (f32[128,128]{1,0:T(8,128)S(1)}, f32[128,128]{1,0:T(8,128)S(1)}, u32[]{:S(2)}, u32[]{:S(2)}) collective-permute-start(f32[128,128]{1,0:T(8,128)S(1)} %constant_dynamic-slice_fusion.1), channel_id=1, source_target_pairs={{0,4},{4,0},{1,5},{5,1},{2,6},{6,2},{3,7},{7,3},{8,12},{12,8},{9,1... | collective-permute-start | bytes 196616 | tf_op jit(solution)/shard_map/ppermute | solution.py:29
  44.9 6.5 %copy-start.7 = (f32[3,256]{1,0:T(4,128)S(1)}, f32[3,256]{1,0:T(4,128)}, u32[]{:S(2)}) copy-start(f32[3,256]{1,0:T(4,128)} %param.21) | copy-start | bytes 9220
  46.0 9.2 %collective-permute-start.1 = (bf16[128,2048]{0,1:T(8,128)(2,1)S(1)}, bf16[128,2048]{0,1:T(8,128)(2,1)}, u32[]{:S(2)}, u32[]{:S(2)}) collective-permute-start(bf16[128,2048]{0,1:T(8,128)(2,1)S(1)} %bitcast.98), channel_id=1, source_target_pairs={{0,4},{4,0},{1,5},{5,1},{2,6},{6,2},{3,7},{7,3},{8,12},{12,8},{9,1... | collective-permute-start | bytes 1572872 | tf_op jit(solution)/shard_map/ppermute | solution.py:29
  51.5 3.5 %collective-permute-start = (bf16[16,2048]{1,0:T(8,128)(2,1)S(1)}, bf16[16,2048]{1,0:T(8,128)(2,1)S(1)}, u32[]{:S(2)}, u32[]{:S(2)}) collective-permute-start(bf16[16,2048]{1,0:T(8,128)(2,1)S(1)} %bitcast.102), channel_id=1, source_target_pairs={{0,4},{4,8},{8,12},{12,16},{16,20},{20,24},{24,28},{28,32},{32,36}... | collective-permute-start | bytes 196616 | tf_op jit(solution)/shard_map/ppermute | solution.py:34
  83.3 3.6 %copy-start.9 = (bf16[2048,1536]{1,0:T(8,128)(2,1)S(1)}, bf16[2048,1536]{1,0:T(8,128)(2,1)}, u32[]{:S(2)}) copy-start(bf16[2048,1536]{1,0:T(8,128)(2,1)} %all-gather.2.cloned.1.call-done) | copy-start | bytes 18874372
  88.1 29.7 %copy-start.2 = (bf16[144,1024]{1,0:T(8,128)(2,1)}, bf16[144,1024]{1,0:T(8,128)(2,1)S(1)}, u32[]{:S(2)}) copy-start(bf16[144,1024]{1,0:T(8,128)(2,1)S(1)} %fusion.5) | copy-start | bytes 884740
  91.5 18.9 %all-to-all-start.2 = ((bf16[8,144,128]{2,1,0:T(8,128)(2,1)}), bf16[8,144,128]{2,1,0:T(8,128)(2,1)S(1)}, u32[]{:S(2)}, u32[]{:S(2)}) async-start(bf16[8,144,128]{2,1,0:T(8,128)(2,1)} %broadcast_in_dim.107), calls=%async_computation.2 | async-start | bytes 589824 | tf_op jit(solution)/shard_map/all_to_all | solution.py:21
  112.4 15.2 %all-to-all-start.3 = ((bf16[8,144,128]{2,1,0:T(8,128)(2,1)}), bf16[8,144,128]{2,1,0:T(8,128)(2,1)S(1)}, u32[]{:S(2)}, u32[]{:S(2)}) async-start(bf16[8,144,128]{2,1,0:T(8,128)(2,1)} %broadcast_in_dim.111), calls=%async_computation.3 | async-start | bytes 589824 | tf_op jit(solution)/shard_map/all_to_all | solution.py:21
  127.9 9.4 %copy-start.1 = (bf16[256,2048]{1,0:T(8,128)(2,1)S(1)}, bf16[256,2048]{1,0:T(8,128)(2,1)}, u32[]{:S(2)}) copy-start(bf16[256,2048]{1,0:T(8,128)(2,1)} %param.30) | copy-start | bytes 3145732
Sparse Core Ops, SparseCore 0:
  30.2 53.0 all-gather.1

commit v2 on v1

--- a/solution.py
+++ b/solution.py
@@ -100,11 +100,13 @@
     w_out_rec,
 ):
     z, y, c = (lax.axis_index(a) for a in SP)
-    own_rows = jnp.concatenate(
-        [retention_gate_matrix, w_input, w_query, w_filter_b, w_filter_c, w_filter_v], axis=1
-    )
-    along_y = sent_to_all(own_rows, "sp_1").reshape(-1, own_rows.shape[1])
-    weights = lax.all_gather(along_y, ("sp_0", "sp_2"), axis=0, tiled=True)
+    state_rows = jnp.concatenate([retention_gate_matrix, w_input], axis=1)
+    state_along_y = sent_to_all(state_rows, "sp_1").reshape(-1, state_rows.shape[1])
+    rest_rows = jnp.concatenate([w_query, w_filter_b, w_filter_c, w_filter_v], axis=1)
+    state_along_y, rest_rows = lax.optimization_barrier((state_along_y, rest_rows))
+    state_weights = lax.all_gather(state_along_y, ("sp_0", "sp_2"), axis=0, tiled=True)
+    rest_along_y = sent_to_all(rest_rows, "sp_1").reshape(-1, rest_rows.shape[1])
+    rest_weights = lax.all_gather(rest_along_y, ("sp_0", "sp_2"), axis=0, tiled=True)
 
     gathered = sent_to_all(tokens, "tp").reshape(-1, tokens.shape[1])
     widened = gathered.astype(f32)
@@ -130,8 +132,10 @@
     head = lambda a, k: lax.dynamic_slice_in_dim(a, k * HEAD_DIM, HEAD_DIM, axis=1)
     partner_fade = swapped(head(fade, 1 - c), "sp_2")
 
+    partner, halo, partner_fade = lax.optimization_barrier((partner, halo, partner_fade))
+
     chip = jnp.concatenate([own, partner], axis=0)
-    chip_gates = jnp.dot(chip, weights[:, :512], preferred_element_type=f32).astype(bf16)
+    chip_gates = jnp.dot(chip, state_weights, preferred_element_type=f32).astype(bf16)
     forget_logit, input_value = chip_gates[:, :256], chip_gates[:, 256:]
     key_rate, log_decay = rates(forget_logit[:length], forget_gap, fade)
     value_in = silu(input_value[:length])
@@ -165,7 +169,7 @@
     incoming = exchanged(jnp.stack([into_chip, into_second]).astype(bf16), "sp_2")
 
     rest = jnp.dot(
-        jnp.concatenate([halo, own], axis=0), weights[:, 512:], preferred_element_type=f32
+        jnp.concatenate([halo, own], axis=0), rest_weights, preferred_element_type=f32
     ).astype(bf16)
     queries = rest[HALO:, :256].astype(f32)
     gate_out = rest[HALO:, 256:512].astype(f32)

time: 159 us -> 147 us (0.925)
  starting transfers between devices: 27.8 us -> 43.3 us
  blocking collectives: 37 us -> 24.2 us
  waiting for transfers between devices: 53.3 us -> 45 us
  local copies, waits for them, and re-layouts: 10.7 us -> 6.35 us
    all_gather x1 -> x2, waiting for transfers between devices: 28 us -> 0.01 us  [the longest x1 0.01 us: body(): lax.all_gather(state_along_y, ('sp_0', 'sp_2'), axis=0, tiled=True)]
    all_to_all x3 -> x5, starting transfers between devices: 15.8 us -> 31.8 us  [exchanged(): return lax.all_to_all(blocks, axis, split_axis=0, concat_axis=0, tiled=True)]
    all_to_all x3 -> x5, waiting for transfers between devices: 24 us -> 39 us  [exchanged(): return lax.all_to_all(blocks, axis, split_axis=0, concat_axis=0, tiled=True)]
    all_to_all x3 -> x2, blocking collectives: 37 us -> 24.2 us  [exchanged(): return lax.all_to_all(blocks, axis, split_axis=0, concat_axis=0, tiled=True)]
    ppermute x1, waiting for transfers between devices: 1.3 us -> 6 us  [shifted(): return lax.ppermute(block, axis, [(i, i + 1) for i in range(size - 1)])]
    unnamed x27 -> x21, local copies, waits for them, and re-layouts: 4.51 us -> 0.81 us
    dot_general x2, matrix products: 3.89 us -> 5.96 us  [the longest x1 3.63 us: body(): jnp.dot(jnp.concatenate([halo, own], axis=0), rest_weights, preferred_ele...]
    broadcast_in_dim x4 -> x5, local copies, waits for them, and re-layouts: 3.29 us -> 3.92 us  [sent_to_all(): return exchanged(jnp.broadcast_to(x, (lax.axis_size(axis), *x.shape)), axis)]
  transfers between devices with their start and end apart: 7 -> 10, of which waited for: 5 -> 5; matrix products, arithmetic and copies ran while one was open for 7% -> 11% of each run, Pallas kernels for 0% -> 0%
where the time goes in v2:
time: 147 us; the launch traced here: 146 us
  waiting for transfers between devices  45 us (31%)
  starting transfers between devices  43.3 us (29%)
  blocking collectives  24.2 us (16%)
  between operations  14 us (10%)
  matrix products  8.89 us (6%)
  local copies, waits for them, and re-layouts  6.35 us (4%)
  other arithmetic  4.52 us (3%)
    all_to_all x5, waiting for transfers between devices, exchanged(): return lax.all_to_all(blocks, axis, split_axis=0, concat_axis=0, tiled=True)  39 us
    all_to_all x5, starting transfers between devices, exchanged(): return lax.all_to_all(blocks, axis, split_axis=0, concat_axis=0, tiled=True)  31.8 us
    all_to_all x2, blocking collectives, exchanged(): return lax.all_to_all(blocks, axis, split_axis=0, concat_axis=0, tiled=True)  24.2 us
    ppermute x2, starting transfers between devices, swapped(): return lax.ppermute(x, axis, [(0, 1), (1, 0)])  9.23 us
    ppermute x1, waiting for transfers between devices, shifted(): return lax.ppermute(block, axis, [(i, i + 1) for i in range(size - 1)])  6 us
    broadcast_in_dim x5, local copies, waits for them, and re-layouts, sent_to_all(): return exchanged(jnp.broadcast_to(x, (lax.axis_size(axis), *x.shape)), axis)  3.92 us
    dot_general x1, matrix products, body(): jnp.dot(jnp.concatenate([halo, own], axis=0), rest_weights, preferred_ele...  3.63 us
  transfers between devices with their start and end apart: 10, of which 5 were waited for; matrix products, arithmetic and copies ran while one was open for 11% of the time, Pallas kernels for 0%

profile of v2, /device:TPU:1, one launch (start us, length us, event | category | flops | bytes accessed | tf_op | source)
XLA Modules:
  0.0 146.2 jit_solution(1586218448661395669)
XLA Ops:
  6.5 0.8 pad_maximum_fusion.2
  7.4 0.7 broadcast_in_dim.105
  8.0 7.6 %all-to-all-start.1 = ((bf16[8,16,512]{2,1,0:T(8,128)(2,1)}), bf16[8,16,512]{2,1,0:T(8,128)(2,1)S(1)}, u32[]{:S(2)}, u32[]{:S(2)}) async-start(bf16[8,16,512]{2,1,0:T(8,128)(2,1)} %broadcast_in_dim.105), calls=%async_computation.1 | async-start | bytes 262144 | tf_op jit(solution)/shard_map/all_to_all | solution.py:21
  15.7 0.8 pad_maximum_fusion.1
  16.5 7.2 %all-to-all-done.1 = bf16[8,16,512]{2,1,0:T(8,128)(2,1)S(1)} async-done(((bf16[8,16,512]{2,1,0:T(8,128)(2,1)}), bf16[8,16,512]{2,1,0:T(8,128)(2,1)S(1)}, u32[]{:S(2)}, u32[]{:S(2)}) %all-to-all-start.1) | async-done | bytes 131104 | tf_op jit(solution)/shard_map/all_to_all | solution.py:21
  24.5 12.6 %all_to_all.35 = bf16[8,16,1024]{2,1,0:T(8,128)(2,1)} all-to-all(bf16[8,16,1024]{2,1,0:T(8,128)(2,1)S(1)} %broadcast_in_dim.106), channel_id=1, replica_groups=mesh['sp_0'=8,'sp_1'=8,'sp_2'=2,'tp'=4] {'sp_1'}, dimensions={0} | all-to-all | bytes 524288 | tf_op jit(solution)/shard_map/all_to_all | solution.py:21
  37.1 1.8 %broadcast_in_dim.104 = bf16[4,32,2048]{2,1,0:T(8,128)(2,1)} broadcast(bf16[32,2048]{1,0:T(8,128)(2,1)} %param.16), dimensions={1,2} | broadcast | bytes 655360 | tf_op jit(solution)/shard_map/broadcast_in_dim | solution.py:25
  38.8 3.7 %all-to-all-start = ((bf16[4,32,2048]{2,1,0:T(8,128)(2,1)}), bf16[4,32,2048]{2,1,0:T(8,128)(2,1)S(1)}, u32[]{:S(2)}, u32[]{:S(2)}) async-start(bf16[4,32,2048]{2,1,0:T(8,128)(2,1)} %broadcast_in_dim.104), calls=%async_computation | async-start | bytes 1048576 | tf_op jit(solution)/shard_map/all_to_all | solution.py:21
  42.5 6.9 %all-to-all-done = bf16[4,32,2048]{2,1,0:T(8,128)(2,1)S(1)} async-done(((bf16[4,32,2048]{2,1,0:T(8,128)(2,1)}), bf16[4,32,2048]{2,1,0:T(8,128)(2,1)S(1)}, u32[]{:S(2)}, u32[]{:S(2)}) %all-to-all-start) | async-done | bytes 524320 | tf_op jit(solution)/shard_map/all_to_all | solution.py:21
  50.7 7.3 %collective-permute-start = (bf16[128,2048]{0,1:T(8,128)(2,1)S(1)}, bf16[128,2048]{0,1:T(8,128)(2,1)S(1)}, u32[]{:S(2)}, u32[]{:S(2)}) collective-permute-start(bf16[128,2048]{0,1:T(8,128)(2,1)S(1)} %bitcast.100), channel_id=1, source_target_pairs={{0,4},{4,0},{1,5},{5,1},{2,6},{6,2},{3,7},{7,3},{8,12},{12,8},{9,1... | collective-permute-start | bytes 1572872 | tf_op jit(solution)/shard_map/ppermute | solution.py:29
  58.0 1.9 %collective-permute-start.2 = (f32[128,128]{1,0:T(8,128)S(1)}, f32[128,128]{1,0:T(8,128)S(1)}, u32[]{:S(2)}, u32[]{:S(2)}) collective-permute-start(f32[128,128]{1,0:T(8,128)S(1)} %constant_dynamic-slice_fusion.1), channel_id=1, source_target_pairs={{0,4},{4,0},{1,5},{5,1},{2,6},{6,2},{3,7},{7,3},{8,12},{12,8},{9,1... | collective-permute-start | bytes 196616 | tf_op jit(solution)/shard_map/ppermute | solution.py:29
  60.3 2.2 %collective-permute-start.1 = (bf16[16,2048]{0,1:T(8,128)(2,1)S(1)}, bf16[16,2048]{0,1:T(8,128)(2,1)}, u32[]{:S(2)}, u32[]{:S(2)}) collective-permute-start(bf16[16,2048]{0,1:T(8,128)(2,1)S(1)} %bitcast.99), channel_id=1, source_target_pairs={{0,4},{4,8},{8,12},{12,16},{16,20},{20,24},{24,28},{28,32},{32,36}... | collective-permute-start | bytes 196616 | tf_op jit(solution)/shard_map/ppermute | solution.py:34
  62.6 6.0 %collective-permute-done.1 = bf16[16,2048]{0,1:T(8,128)(2,1)} collective-permute-done((bf16[16,2048]{0,1:T(8,128)(2,1)S(1)}, bf16[16,2048]{0,1:T(8,128)(2,1)}, u32[]{:S(2)}, u32[]{:S(2)}) %collective-permute-start.1) | collective-permute-done | bytes 65568 | tf_op jit(solution)/shard_map/ppermute | solution.py:34
  68.6 2.3 %convolution_convert_fusion.2 = bf16[256,512]{1,0:T(8,128)(2,1)S(1)} fusion(bf16[2048,512]{1,0:T(8,128)(2,1)} %all-gather.5.cloned.1.call-done, bf16[128,2048]{0,1:T(8,128)(2,1)S(1)} %collective-permute-done, bf16[128,2048]{0,1:T(8,128)(2,1)S(1)} %bitcast.101), kind=kOutput, calls=%fused_computation.4 | convolution fusion | flops 539099136 | bytes 3407872 | tf_op jit(solution)/shard_map/dot_general | solution.py:138
  72.3 0.7 broadcast_in_dim.111
  73.0 6.4 %all-to-all-start.3 = ((bf16[8,144,128]{2,1,0:T(8,128)(2,1)}), bf16[8,144,128]{2,1,0:T(8,128)(2,1)S(1)}, u32[]{:S(2)}, u32[]{:S(2)}) async-start(bf16[8,144,128]{2,1,0:T(8,128)(2,1)} %broadcast_in_dim.111), calls=%async_computation.3 | async-start | bytes 589824 | tf_op jit(solution)/shard_map/all_to_all | solution.py:21
  79.6 12.7 %all-to-all-done.3 = bf16[8,144,128]{2,1,0:T(8,128)(2,1)S(1)} async-done(((bf16[8,144,128]{2,1,0:T(8,128)(2,1)}), bf16[8,144,128]{2,1,0:T(8,128)(2,1)S(1)}, u32[]{:S(2)}, u32[]{:S(2)}) %all-to-all-start.3) | async-done | bytes 294944 | tf_op jit(solution)/shard_map/all_to_all | solution.py:21
  92.9 0.7 broadcast_in_dim.115
  93.7 4.9 %all-to-all-start.4 = ((bf16[8,144,128]{2,1,0:T(8,128)(2,1)}), bf16[8,144,128]{2,1,0:T(8,128)(2,1)S(1)}, u32[]{:S(2)}, u32[]{:S(2)}) async-start(bf16[8,144,128]{2,1,0:T(8,128)(2,1)} %broadcast_in_dim.115), calls=%async_computation.4 | async-start | bytes 589824 | tf_op jit(solution)/shard_map/all_to_all | solution.py:21
  99.2 12.1 %all-to-all-done.4 = bf16[8,144,128]{2,1,0:T(8,128)(2,1)S(1)} async-done(((bf16[8,144,128]{2,1,0:T(8,128)(2,1)}), bf16[8,144,128]{2,1,0:T(8,128)(2,1)S(1)}, u32[]{:S(2)}, u32[]{:S(2)}) %all-to-all-start.4) | async-done | bytes 294944 | tf_op jit(solution)/shard_map/all_to_all | solution.py:21
  112.2 9.1 %all-to-all-start.5 = ((bf16[2,128,128]{2,1,0:T(8,128)(2,1)}), bf16[2,128,128]{2,1,0:T(8,128)(2,1)S(1)}, u32[]{:S(2)}, u32[]{:S(2)}) async-start(bf16[2,128,128]{2,1,0:T(8,128)(2,1)} %pad_maximum_fusion), calls=%async_computation.5 | async-start | bytes 131072 | tf_op jit(solution)/shard_map/all_to_all | solution.py:21
  121.4 3.6 %convolution_convert_fusion.1 = bf16[144,1024]{1,0:T(8,128)(2,1)S(1)} fusion(bf16[2048,1024]{1,0:T(8,128)(2,1)} %all-gather.3.cloned.1.call-done, bf16[128,2048]{0,1:T(8,128)(2,1)S(1)} %bitcast.102, bf16[16,2048]{0,1:T(8,128)(2,1)} %collective-permute-done.1), kind=kOutput, calls=%fused_computation.3 | convolution fusion | flops 605306880 | bytes 5079040 | tf_op jit(solution)/shard_map/dot_general | solution.py:171
  127.0 11.6 %all_to_all.36 = bf16[4,32,2048]{2,1,0:T(8,128)(2,1)S(1)} all-to-all(bf16[4,32,2048]{2,1,0:T(8,128)(2,1)S(1)} %bitcast.95), channel_id=1, replica_groups=mesh['sp_0'=8,'sp_1'=8,'sp_2'=2,'tp'=4] {'tp'}, dimensions={0} | all-to-all | bytes 1048576 | tf_op jit(solution)/shard_map/all_to_all | solution.py:21
  138.7 0.7 reduce_sum.145
  (105 shorter events, 7.7 us)
Async XLA Ops:
  6.5 119.8 %copy-start = (bf16[256,2048]{1,0:T(8,128)(2,1)S(1)}, bf16[256,2048]{1,0:T(8,128)(2,1)}, u32[]{:S(2)}) copy-start(bf16[256,2048]{1,0:T(8,128)(2,1)} %param.29) | copy-start | bytes 3145732
  6.5 36.0 %copy-start.6 = (f32[2048]{0:T(1024)S(1)}, f32[2048]{0:T(1024)}, u32[]{:S(2)}) copy-start(f32[2048]{0:T(1024)} %param.17) | copy-start | bytes 24580
  8.0 15.7 %all-to-all-start.1 = ((bf16[8,16,512]{2,1,0:T(8,128)(2,1)}), bf16[8,16,512]{2,1,0:T(8,128)(2,1)S(1)}, u32[]{:S(2)}, u32[]{:S(2)}) async-start(bf16[8,16,512]{2,1,0:T(8,128)(2,1)} %broadcast_in_dim.105), calls=%async_computation.1 | async-start | bytes 262144 | tf_op jit(solution)/shard_map/all_to_all | solution.py:21
  15.7 52.9 %all-gather.5.cloned.1.call-start = ((), (), s32[]{:S(2)}) async-start(), calls=%async_computation.8 | async-start | bytes 2228224 | tf_op jit(solution)/shard_map/all_gather | solution.py:107
  23.7 0.7 copy-start.2
  24.4 97.0 %all-gather.3.cloned.1.call-start = ((), (), s32[]{:S(2)}) async-start(), calls=%async_computation.7 | async-start | bytes 4456448 | tf_op jit(solution)/shard_map/all_gather | solution.py:109
  38.8 10.6 %all-to-all-start = ((bf16[4,32,2048]{2,1,0:T(8,128)(2,1)}), bf16[4,32,2048]{2,1,0:T(8,128)(2,1)S(1)}, u32[]{:S(2)}, u32[]{:S(2)}) async-start(bf16[4,32,2048]{2,1,0:T(8,128)(2,1)} %broadcast_in_dim.104), calls=%async_computation | async-start | bytes 1048576 | tf_op jit(solution)/shard_map/all_to_all | solution.py:21
  42.5 7.6 %copy-start.4 = (bf16[256,256,1]{1,0,2:T(8,128)(2,1)S(1)}, bf16[256,256,1]{1,0,2:T(8,128)(2,1)}, u32[]{:S(2)}) copy-start(bf16[256,256,1]{1,0,2:T(8,128)(2,1)} %constant.72) | copy-start | bytes 393220
  49.6 8.5 %copy-start.3 = (f32[128,256]{1,0:T(8,128)S(1)}, f32[128,256]{1,0:T(8,128)}, u32[]{:S(2)}) copy-start(f32[128,256]{1,0:T(8,128)} %param.26) | copy-start | bytes 393220
  49.8 12.7 %copy-start.8 = (f32[256]{0:T(256)S(1)}, f32[256]{0:T(256)}, u32[]{:S(2)}) copy-start(f32[256]{0:T(256)} %param.25) | copy-start | bytes 3076
  50.7 17.9 %collective-permute-start = (bf16[128,2048]{0,1:T(8,128)(2,1)S(1)}, bf16[128,2048]{0,1:T(8,128)(2,1)S(1)}, u32[]{:S(2)}, u32[]{:S(2)}) collective-permute-start(bf16[128,2048]{0,1:T(8,128)(2,1)S(1)} %bitcast.100), channel_id=1, source_target_pairs={{0,4},{4,0},{1,5},{5,1},{2,6},{6,2},{3,7},{7,3},{8,12},{12,8},{9,1... | collective-permute-start | bytes 1572872 | tf_op jit(solution)/shard_map/ppermute | solution.py:29
  58.0 4.6 %collective-permute-start.2 = (f32[128,128]{1,0:T(8,128)S(1)}, f32[128,128]{1,0:T(8,128)S(1)}, u32[]{:S(2)}, u32[]{:S(2)}) collective-permute-start(f32[128,128]{1,0:T(8,128)S(1)} %constant_dynamic-slice_fusion.1), channel_id=1, source_target_pairs={{0,4},{4,0},{1,5},{5,1},{2,6},{6,2},{3,7},{7,3},{8,12},{12,8},{9,1... | collective-permute-start | bytes 196616 | tf_op jit(solution)/shard_map/ppermute | solution.py:29
  60.3 8.4 %collective-permute-start.1 = (bf16[16,2048]{0,1:T(8,128)(2,1)S(1)}, bf16[16,2048]{0,1:T(8,128)(2,1)}, u32[]{:S(2)}, u32[]{:S(2)}) collective-permute-start(bf16[16,2048]{0,1:T(8,128)(2,1)S(1)} %bitcast.99), channel_id=1, source_target_pairs={{0,4},{4,8},{8,12},{12,16},{16,20},{20,24},{24,28},{28,32},{32,36}... | collective-permute-start | bytes 196616 | tf_op jit(solution)/shard_map/ppermute | solution.py:34
  70.9 8.5 %copy-start.5 = (f32[2,128,128]{2,1,0:T(8,128)S(1)}, f32[2,128,128]{2,1,0:T(8,128)}, u32[]{:S(2)}) copy-start(f32[2,128,128]{2,1,0:T(8,128)} %param.28) | copy-start | bytes 393220
  71.4 27.2 %copy-start.7 = (f32[3,256]{1,0:T(4,128)S(1)}, f32[3,256]{1,0:T(4,128)}, u32[]{:S(2)}) copy-start(f32[3,256]{1,0:T(4,128)} %param.21) | copy-start | bytes 9220
  73.0 19.3 %all-to-all-start.3 = ((bf16[8,144,128]{2,1,0:T(8,128)(2,1)}), bf16[8,144,128]{2,1,0:T(8,128)(2,1)S(1)}, u32[]{:S(2)}, u32[]{:S(2)}) async-start(bf16[8,144,128]{2,1,0:T(8,128)(2,1)} %broadcast_in_dim.111), calls=%async_computation.3 | async-start | bytes 589824 | tf_op jit(solution)/shard_map/all_to_all | solution.py:21
  93.7 17.5 %all-to-all-start.4 = ((bf16[8,144,128]{2,1,0:T(8,128)(2,1)}), bf16[8,144,128]{2,1,0:T(8,128)(2,1)S(1)}, u32[]{:S(2)}, u32[]{:S(2)}) async-start(bf16[8,144,128]{2,1,0:T(8,128)(2,1)} %broadcast_in_dim.115), calls=%async_computation.4 | async-start | bytes 589824 | tf_op jit(solution)/shard_map/all_to_all | solution.py:21
  112.2 13.6 %all-to-all-start.5 = ((bf16[2,128,128]{2,1,0:T(8,128)(2,1)}), bf16[2,128,128]{2,1,0:T(8,128)(2,1)S(1)}, u32[]{:S(2)}, u32[]{:S(2)}) async-start(bf16[2,128,128]{2,1,0:T(8,128)(2,1)} %pad_maximum_fusion), calls=%async_computation.5 | async-start | bytes 131072 | tf_op jit(solution)/shard_map/all_to_all | solution.py:21
  125.0 1.1 copy-start.9
  125.2 1.5 copy-start.1
Sparse Core Ops, SparseCore 0:
  24.5 43.9 all-gather.4
  70.6 46.6 all-gather.2

commit v3 on v2

v3 whole, which is shorter than its diff:
```python
import jax
import jax.numpy as jnp
import numpy as np
from jax import lax
from jax.experimental import pallas as pl
from jax.experimental.pallas import tpu as pltpu
from jax.sharding import Mesh
from jax.sharding import PartitionSpec as P

HEAD_DIM = 128
SPAN = 64
TAPS = 3
HALO = 16
SP = ("sp_0", "sp_1", "sp_2")
SP_TP = ("sp_0", "sp_1", "sp_2", "tp")

epsilon = 1e-06
f32 = jnp.float32
bf16 = jnp.bfloat16


def exchanged(blocks, axis):
    return lax.all_to_all(blocks, axis, split_axis=0, concat_axis=0, tiled=True)


def sent_to_all(x, axis):
    return exchanged(jnp.broadcast_to(x, (lax.axis_size(axis), *x.shape)), axis)


def swapped(x, axis):
    return lax.ppermute(x, axis, [(0, 1), (1, 0)])


def shifted(block, axis):
    size = lax.axis_size(axis)
    return lax.ppermute(block, axis, [(i, i + 1) for i in range(size - 1)])


HIGHEST = lax.Precision.HIGHEST
ANY = pl.BlockSpec(memory_space=pl.ANY)
VMEM = pl.BlockSpec(memory_space=pltpu.VMEM)
SMEM = pl.BlockSpec(memory_space=pltpu.SMEM)
PIECES = 4
RATE, RUNNING, VALUE, STATE_0, INITIAL, DECAY_0, CARRIED = 0, 2, 4, 6, 7, 8, 9


def contracted(a, b, over):
    return lax.dot_general(a, b, ((over[0:1], over[1:2]), ((), ())), preferred_element_type=f32)


def running_sum(x):
    size = x.shape[0]
    row = lax.broadcasted_iota(jnp.int32, (size, size), 0)
    column = lax.broadcasted_iota(jnp.int32, (size, size), 1)
    causal = jnp.where(column <= row, 1.0, 0.0).astype(f32)
    return jnp.dot(causal, x, precision=HIGHEST, preferred_element_type=f32)


def sigmoid(v):
    return 1.0 / (1.0 + jnp.exp(-v))


def packed_rows(decay, state):
    high = decay.astype(bf16).astype(f32)
    rest = decay - high
    low = rest.astype(bf16).astype(f32)
    place = lax.broadcasted_iota(jnp.int32, (16, HEAD_DIM), 0)
    tail = jnp.where(place == 0, high, jnp.where(place == 1, low, rest - low))
    tail = jnp.where(place < 3, tail, 0.0)
    return jnp.concatenate([state, tail], axis=0).astype(bf16)


def state_kernel(
    core, own, partner, weights, gap, fade, partner_fade, initial,
    packed, carried,
    held, fade_held, initial_held, sems, small_sems,
):
    length = own.shape[0]
    piece = weights.shape[0] // PIECES
    copies = [
        pltpu.make_async_copy(weights.at[pl.ds(k * piece, piece)], held.at[k], sems.at[k])
        for k in range(PIECES)
    ]
    small_copies = [
        pltpu.make_async_copy(partner_fade, fade_held, small_sems.at[0]),
        pltpu.make_async_copy(initial.at[core[0]], initial_held, small_sems.at[1]),
    ]
    for copy in copies + small_copies:
        copy.start()
    rows = jnp.concatenate([own[...], partner[...]], axis=0)
    total = jnp.zeros((2 * length, weights.shape[1]), f32)
    for k in range(PIECES):
        copies[k].wait()
        total = total + jnp.dot(
            rows[:, k * piece : (k + 1) * piece], held[k], preferred_element_type=f32
        )
    for copy in small_copies:
        copy.wait()
    logits = total.astype(bf16).astype(f32)
    first = core[0] == 0

    def head(a):
        return jnp.where(first, a[:, :HEAD_DIM], a[:, HEAD_DIM:])

    wide = 2 * HEAD_DIM
    rate = gap[...] * sigmoid(-logits[:length, :wide])
    fall = jnp.log1p(-rate) + fade[...]
    value = logits[:length, wide:] * sigmoid(logits[:length, wide:])
    partner_rate = head(gap[...]) * sigmoid(-head(logits[length:, :wide]))
    partner_fall = jnp.log1p(-partner_rate) + fade_held[...]
    partner_value = head(logits[length:, wide:])
    partner_value = partner_value * sigmoid(partner_value)
    summed = running_sum(jnp.concatenate([fall, partner_fall], axis=1))
    running = summed[:, :wide]
    for h in range(2):
        cut = slice(h * HEAD_DIM, (h + 1) * HEAD_DIM)
        carried[RATE + h] = rate[:, cut]
        carried[RUNNING + h] = running[:, cut]
        carried[VALUE + h] = value[:, cut]
    carried[INITIAL] = initial_held[...].T

    def state_of(key, run, val):
        remainder = (key * jnp.exp(run[length - 1 :] - run)).astype(bf16)
        return run[length - 1 :], contracted(val.T.astype(bf16), remainder, (1, 0))

    own_decay, own_state = state_of(head(rate), head(running), head(value))
    next_decay, next_state = state_of(partner_rate, summed[:, wide:], partner_value)
    d0 = jnp.where(first, own_decay, next_decay)
    d1 = jnp.where(first, next_decay, own_decay)
    s0 = jnp.where(first, own_state, next_state)
    s1 = jnp.where(first, next_state, own_state)
    carried[DECAY_0, 0:1] = d0
    carried[STATE_0] = s0
    out = packed_rows(d0 + d1, jnp.exp(d1) * s0 + s1)
    for k in range(packed.shape[0]):
        packed[k] = out


def decay_at(arrived, k):
    tail = arrived[k, HEAD_DIM : HEAD_DIM + 16].astype(f32)
    place = lax.broadcasted_iota(jnp.int32, tail.shape, 0)
    return jnp.sum(jnp.where(place < 3, tail, 0.0), axis=0, keepdims=True)


def before_place(arrived, place):
    decay = jnp.zeros((1, HEAD_DIM), f32)
    state = jnp.zeros((HEAD_DIM, HEAD_DIM), f32)
    for k in reversed(range(arrived.shape[0])):
        weight = jnp.where(k < place, jnp.exp(decay), 0.0)
        state = state + weight * arrived[k, :HEAD_DIM].astype(f32)
        decay = decay + jnp.where(k < place, decay_at(arrived, k), 0.0)
    return decay, state


def row_kernel(place, arrived, carried, packed, decays, states):
    decay, state = before_place(arrived, arrived.shape[0])
    out = packed_rows(decay, state)
    for k in range(packed.shape[0]):
        packed[k] = out
    decay, state = before_place(arrived, place[0])
    decay_0 = carried[DECAY_0, 0:1]
    decays[0:1] = decay
    decays[1:2] = decay + decay_0
    states[0] = state
    states[1] = jnp.exp(decay_0) * state + carried[STATE_0]


def enter_kernel(place, arrived, carried, decays, states, incoming):
    decay, state = before_place(arrived, place[0])
    before = jnp.exp(decay) * carried[INITIAL] + state
    for k in range(2):
        incoming[k] = (jnp.exp(decays[k : k + 1]) * before + states[k]).astype(bf16)


def final_kernel(
    halo, own, weights, carried, taps, incoming, head_gain, w_filter, w_rec,
    partial,
    held, rows, out_filter, out_rec, sems, row_sems, out_sems,
):
    length = own.shape[0]
    piece = weights.shape[0] // PIECES
    row_copies = [
        pltpu.make_async_copy(halo, rows.at[pl.ds(0, HALO)], row_sems.at[0]),
        pltpu.make_async_copy(own, rows.at[pl.ds(HALO, length)], row_sems.at[1]),
    ]
    out_copies = [
        pltpu.make_async_copy(w_filter, out_filter, out_sems.at[0]),
        pltpu.make_async_copy(w_rec, out_rec, out_sems.at[1]),
    ]
    for copy in row_copies:
        copy.start()
    copies = [
        pltpu.make_async_copy(weights.at[pl.ds(k * piece, piece)], held.at[k], sems.at[k])
        for k in range(PIECES)
    ]
    for copy in copies + out_copies:
        copy.start()
    for copy in row_copies:
        copy.wait()
    total = jnp.zeros((HALO + length, weights.shape[1]), f32)
    for k in range(PIECES):
        copies[k].wait()
        total = total + jnp.dot(
            rows[:, k * piece : (k + 1) * piece], held[k], preferred_element_type=f32
        )
    wide = 2 * HEAD_DIM
    rest = total.astype(bf16).astype(f32)
    product = rest[:, 2 * wide : 3 * wide] * rest[:, 3 * wide :]
    filtered = taps[TAPS - 1 : TAPS] * product
    for back in range(1, TAPS):
        at = TAPS - 1 - back
        filtered = filtered + taps[at : at + 1] * pltpu.roll(product, back, 0)
    filter_out = (rest[:, wide : 2 * wide] * filtered)[HALO:].astype(bf16)
    queries = rest[HALO:, :wide]
    mean = 1.0 / HEAD_DIM
    row = lax.broadcasted_iota(jnp.int32, (SPAN, SPAN), 0)
    column = lax.broadcasted_iota(jnp.int32, (SPAN, SPAN), 1)
    parts = []
    for h in range(2):
        cut = slice(h * HEAD_DIM, (h + 1) * HEAD_DIM)
        run = carried[RUNNING + h]
        rate = carried[RATE + h]
        value = carried[VALUE + h].astype(bf16)
        full = (queries[:, cut] * jnp.exp(run)).astype(bf16)
        blocks = []
        edge = jnp.zeros((1, HEAD_DIM), f32)
        earlier = None
        for b in range(length // SPAN):
            at = slice(b * SPAN, (b + 1) * SPAN)
            inside = run[at] - edge
            last = run[(b + 1) * SPAN - 1 : (b + 1) * SPAN]
            scaled_query = (queries[at, cut] * jnp.exp(inside)).astype(bf16)
            scaled_key = (rate[at] * jnp.exp(-inside)).astype(bf16)
            scores = contracted(scaled_query, scaled_key, (1, 1))
            scores = jnp.where(column <= row, scores, 0.0).astype(bf16)
            vals = value[at]
            local = jnp.dot(scores, vals, preferred_element_type=f32)
            if earlier is not None:
                across = contracted(scaled_query, earlier[0], (1, 1)).astype(bf16)
                local = local + jnp.dot(across, earlier[1], preferred_element_type=f32)
            remainder = (rate[at] * jnp.exp(last - run[at])).astype(bf16)
            earlier = (remainder, vals)
            edge = last
            blocks.append(local)
        raw = jnp.concatenate(blocks, axis=0) + contracted(full, incoming[h], (1, 1))
        scale = lax.rsqrt(jnp.sum(raw * raw, axis=-1, keepdims=True) * mean + epsilon)
        parts.append((raw * scale * head_gain[...]).astype(bf16))
    rec_out = jnp.concatenate(parts, axis=1)
    for copy in out_copies:
        copy.wait()
    partial[...] = (
        jnp.dot(filter_out, out_filter[...], preferred_element_type=f32)
        + jnp.dot(rec_out, out_rec[...], preferred_element_type=f32)
    ).astype(bf16)


def made(shape, kind):
    return pltpu.VMEM(shape, kind)


def granted(mebibytes):
    return pltpu.CompilerParams(vmem_limit_bytes=mebibytes * 2**20)


def far(x):
    return pltpu.with_memory_space_constraint(x, pltpu.HBM)


def near(x):
    return pltpu.with_memory_space_constraint(x, pltpu.VMEM)


def body(
    tokens,
    norm_gain,
    w_filter_b,
    w_filter_c,
    w_filter_v,
    filter_taps,
    w_query,
    retention_gate_matrix,
    w_input,
    forget_gap,
    additive_fade_log,
    head_gain,
    initial_state,
    w_out_filter,
    w_out_rec,
):
    z, y, c = (lax.axis_index(a) for a in SP)
    state_rows = jnp.concatenate([retention_gate_matrix, w_input], axis=1)
    state_along_y = sent_to_all(state_rows, "sp_1").reshape(-1, state_rows.shape[1])
    rest_rows = jnp.concatenate([w_query, w_filter_b, w_filter_c, w_filter_v], axis=1)
    state_along_y, rest_rows = lax.optimization_barrier((state_along_y, rest_rows))
    state_weights = lax.all_gather(state_along_y, ("sp_0", "sp_2"), axis=0, tiled=True)
    rest_along_y = sent_to_all(rest_rows, "sp_1").reshape(-1, rest_rows.shape[1])
    rest_weights = lax.all_gather(rest_along_y, ("sp_0", "sp_2"), axis=0, tiled=True)

    gathered = sent_to_all(tokens, "tp").reshape(-1, tokens.shape[1])
    widened = gathered.astype(f32)
    normed = (
        widened
        * lax.rsqrt(jnp.mean(widened * widened, axis=-1, keepdims=True) + epsilon)
        * norm_gain
    ).astype(bf16)
    length, width = normed.shape
    order = np.arange(256).reshape(8, 2, 16).transpose(1, 0, 2).reshape(-1)
    swap = np.zeros((256, 256), np.float32)
    swap[order, np.arange(256)] = 1.0
    own = jnp.einsum(
        "tzk,kl->tzl",
        normed.reshape(length, 8, 256),
        jnp.asarray(swap, bf16),
        preferred_element_type=f32,
    ).astype(bf16).reshape(length, width)
    partner = swapped(own, "sp_2")
    halo = shifted(own[length - HALO :], SP)

    fade = additive_fade_log
    head = lambda a, k: lax.dynamic_slice_in_dim(a, k * HEAD_DIM, HEAD_DIM, axis=1)
    partner_fade = swapped(head(fade, 1 - c), "sp_2")

    partner, halo, partner_fade = lax.optimization_barrier((partner, halo, partner_fade))

    core = jnp.stack([c])
    dma = pltpu.SemaphoreType.DMA
    square = (HEAD_DIM, HEAD_DIM)
    packed_shape = jax.ShapeDtypeStruct((8, HEAD_DIM + 16, HEAD_DIM), bf16)
    packed, carried = pl.pallas_call(
        state_kernel,
        in_specs=[SMEM, VMEM, VMEM, ANY, VMEM, VMEM, ANY, ANY],
        out_specs=[VMEM] * 2,
        out_shape=[packed_shape, made((CARRIED, *square), f32)],
        scratch_shapes=[
            pltpu.VMEM((PIECES, width // PIECES, 512), bf16),
            pltpu.VMEM(square, f32),
            pltpu.VMEM(square, f32),
            dma((PIECES,)),
            dma((2,)),
        ],
        name="chip_state",
        compiler_params=granted(12),
    )(
        core,
        near(own),
        near(partner),
        far(state_weights),
        near(forget_gap[None]),
        near(fade),
        far(partner_fade),
        far(initial_state),
    )

    packed, decays, states = pl.pallas_call(
        row_kernel,
        in_specs=[SMEM] + [VMEM] * 2,
        out_specs=[VMEM] * 3,
        out_shape=[packed_shape, made((8, HEAD_DIM), f32), made((2, *square), f32)],
        name="along_row",
        compiler_params=granted(4),
    )(jnp.stack([y]), near(exchanged(packed, "sp_1")), carried)
    incoming = pl.pallas_call(
        enter_kernel,
        in_specs=[SMEM] + [VMEM] * 4,
        out_specs=VMEM,
        out_shape=made((2, *square), bf16),
        name="enter_chip",
        compiler_params=granted(4),
    )(jnp.stack([z]), near(exchanged(packed, "sp_0")), carried, decays, states)
    incoming = exchanged(incoming, "sp_2")

    partial = pl.pallas_call(
        final_kernel,
        in_specs=[ANY, ANY, ANY] + [VMEM] * 4 + [ANY, ANY],
        out_specs=VMEM,
        out_shape=made((length, width), bf16),
        scratch_shapes=[
            pltpu.VMEM((PIECES, width // PIECES, 1024), bf16),
            pltpu.VMEM((HALO + length, width), bf16),
            pltpu.VMEM((256, width), bf16),
            pltpu.VMEM((256, width), bf16),
            dma((PIECES,)),
            dma((2,)),
            dma((2,)),
        ],
        name="outputs",
        compiler_params=granted(20),
    )(
        far(halo),
        far(own),
        far(rest_weights),
        carried,
        near(filter_taps),
        near(incoming),
        near(head_gain[None]),
        far(w_out_filter),
        far(w_out_rec),
    )
    arrived = exchanged(partial.reshape(4, length // 4, -1), "tp")
    return arrived.astype(f32).sum(axis=0).astype(bf16)


def solution(mesh):
    torus = Mesh(mesh.devices.reshape(8, 8, 2, mesh.shape["tp"]), ("sp_0", "sp_1", "sp_2", "tp"))
    placed = (
        P(SP_TP, None),
        P(),
        P(SP, "tp"),
        P(SP, "tp"),
        P(SP, "tp"),
        P(None, "tp"),
        P(SP, "tp"),
        P(SP, "tp"),
        P(SP, "tp"),
        P("tp"),
        P(SP, "tp"),
        P(),
        P("tp", None, None),
        P("tp", None),
        P("tp", None),
    )
    return jax.shard_map(
        body, mesh=torus, in_specs=placed, out_specs=P(SP_TP, None), check_vma=False
    )
```

time: 147 us -> 144 us (0.980)
  starting transfers between devices: 43.3 us -> 32.9 us
  Pallas kernels: 0 us -> 8.97 us
  matrix products: 8.89 us -> 0.32 us
  blocking collectives: 24.2 us -> 31.3 us
  waiting for transfers between devices: 45 us -> 49.7 us
  local copies, waits for them, and re-layouts: 6.35 us -> 4.09 us
  other arithmetic: 4.52 us -> 2.66 us
    all_to_all x5 -> x4, starting transfers between devices: 31.8 us -> 21.4 us  [exchanged(): return lax.all_to_all(blocks, axis, split_axis=0, concat_axis=0, tiled=True)]
    pallas_call x0 -> x4, Pallas kernels: none -> 8.97 us  [the longest x1 4.56 us: body(): pl.pallas_call(final_kernel, in_specs=[ANY, ANY, ANY] + [VMEM] * 4 + [ANY...]
    dot_general x12 -> x0, matrix products: 8.57 us -> none  [the longest x1 3.63 us: body(): jnp.dot(jnp.concatenate([halo, own], axis=0), rest_weights, preferred_ele...]
    all_to_all x2 -> x3, blocking collectives: 24.2 us -> 31.3 us  [exchanged(): return lax.all_to_all(blocks, axis, split_axis=0, concat_axis=0, tiled=True)]
    all_gather x1, waiting for transfers between devices: 0.01 us -> 5.04 us  [body(): lax.all_gather(state_along_y, ('sp_0', 'sp_2'), axis=0, tiled=True)]
    ppermute x1, waiting for transfers between devices: 6 us -> 1.29 us  [shifted(): return lax.ppermute(block, axis, [(i, i + 1) for i in range(size - 1)])]
    all_to_all x5 -> x4, waiting for transfers between devices: 39 us -> 41.2 us  [exchanged(): return lax.all_to_all(blocks, axis, split_axis=0, concat_axis=0, tiled=True)]
    all_gather x1, waiting for transfers between devices: 0.01 us -> 2.15 us  [body(): lax.all_gather(rest_along_y, ('sp_0', 'sp_2'), axis=0, tiled=True)]
  transfers between devices with their start and end apart: 10 -> 9, of which waited for: 5 -> 7; matrix products, arithmetic and copies ran while one was open for 11% -> 3% of each run, Pallas kernels for 0% -> 3%
where the time goes in v3:
time: 144 us
  waiting for transfers between devices  49.7 us (35%)
  starting transfers between devices  32.9 us (23%)
  blocking collectives  31.3 us (22%)
  between operations  13.6 us (9%)
  Pallas kernels  8.97 us (6%)
  local copies, waits for them, and re-layouts  4.09 us (3%)
  other arithmetic  2.66 us (2%)
    all_to_all x4, waiting for transfers between devices, exchanged(): return lax.all_to_all(blocks, axis, split_axis=0, concat_axis=0, tiled=True)  41.2 us
    all_to_all x3, blocking collectives, exchanged(): return lax.all_to_all(blocks, axis, split_axis=0, concat_axis=0, tiled=True)  31.3 us
    all_to_all x4, starting transfers between devices, exchanged(): return lax.all_to_all(blocks, axis, split_axis=0, concat_axis=0, tiled=True)  21.4 us
    ppermute x2, starting transfers between devices, swapped(): return lax.ppermute(x, axis, [(0, 1), (1, 0)])  9.23 us
    all_gather x1, waiting for transfers between devices, body(): lax.all_gather(state_along_y, ('sp_0', 'sp_2'), axis=0, tiled=True)  5.04 us
    pallas_call x1, Pallas kernels, body(): pl.pallas_call(final_kernel, in_specs=[ANY, ANY, ANY] + [VMEM] * 4 + [ANY...  4.56 us
    pallas_call x1, Pallas kernels, body(): pl.pallas_call(state_kernel, in_specs=[SMEM, VMEM, VMEM, ANY, VMEM, VMEM,...  3.51 us
  transfers between devices with their start and end apart: 9, of which 7 were waited for; matrix products, arithmetic and copies ran while one was open for 3% of the time, Pallas kernels for 3%

profile of v3, /device:TPU:1, one launch (start us, length us, event | category | flops | bytes accessed | tf_op | source)
XLA Modules:
  0.0 143.5 jit_solution(6012937668498696107)
XLA Ops:
  6.5 0.8 pad_maximum_fusion.1
  8.0 7.6 %all-to-all-start.1 = ((bf16[8,16,512]{2,1,0:T(8,128)(2,1)}), bf16[8,16,512]{2,1,0:T(8,128)(2,1)S(1)}, u32[]{:S(2)}, u32[]{:S(2)}) async-start(bf16[8,16,512]{2,1,0:T(8,128)(2,1)} %broadcast_in_dim.18), calls=%async_computation.1 | async-start | bytes 262144 | tf_op jit(solution)/shard_map/all_to_all | solution.py:23
  15.6 0.8 pad_maximum_fusion
  16.4 7.2 %all-to-all-done.1 = bf16[8,16,512]{2,1,0:T(8,128)(2,1)S(1)} async-done(((bf16[8,16,512]{2,1,0:T(8,128)(2,1)}), bf16[8,16,512]{2,1,0:T(8,128)(2,1)S(1)}, u32[]{:S(2)}, u32[]{:S(2)}) %all-to-all-start.1) | async-done | bytes 131104 | tf_op jit(solution)/shard_map/all_to_all | solution.py:23
  24.4 12.7 %all_to_all.35 = bf16[8,16,1024]{2,1,0:T(8,128)(2,1)} all-to-all(bf16[8,16,1024]{2,1,0:T(8,128)(2,1)S(1)} %broadcast_in_dim.19), channel_id=1, replica_groups=mesh['sp_0'=8,'sp_1'=8,'sp_2'=2,'tp'=4] {'sp_1'}, dimensions={0} | all-to-all | bytes 524288 | tf_op jit(solution)/shard_map/all_to_all | solution.py:23
  37.2 1.8 %broadcast_in_dim.17 = bf16[4,32,2048]{2,1,0:T(8,128)(2,1)} broadcast(bf16[32,2048]{1,0:T(8,128)(2,1)} %param.16), dimensions={1,2} | broadcast | bytes 655360 | tf_op jit(solution)/shard_map/broadcast_in_dim | solution.py:27
  38.9 3.7 %all-to-all-start = ((bf16[4,32,2048]{2,1,0:T(8,128)(2,1)}), bf16[4,32,2048]{2,1,0:T(8,128)(2,1)S(1)}, u32[]{:S(2)}, u32[]{:S(2)}) async-start(bf16[4,32,2048]{2,1,0:T(8,128)(2,1)} %broadcast_in_dim.17), calls=%async_computation | async-start | bytes 1048576 | tf_op jit(solution)/shard_map/all_to_all | solution.py:23
  43.3 6.2 %all-to-all-done = bf16[4,32,2048]{2,1,0:T(8,128)(2,1)S(1)} async-done(((bf16[4,32,2048]{2,1,0:T(8,128)(2,1)}), bf16[4,32,2048]{2,1,0:T(8,128)(2,1)S(1)}, u32[]{:S(2)}, u32[]{:S(2)}) %all-to-all-start) | async-done | bytes 524320 | tf_op jit(solution)/shard_map/all_to_all | solution.py:23
  50.6 7.3 %collective-permute-start = (bf16[128,2048]{1,0:T(8,128)(2,1)S(1)}, bf16[128,2048]{1,0:T(8,128)(2,1)S(1)}, u32[]{:S(2)}, u32[]{:S(2)}) collective-permute-start(bf16[128,2048]{1,0:T(8,128)(2,1)S(1)} %bitcast.24), channel_id=1, source_target_pairs={{0,4},{4,0},{1,5},{5,1},{2,6},{6,2},{3,7},{7,3},{8,12},{12,8},{9,1... | collective-permute-start | bytes 1572872 | tf_op jit(solution)/shard_map/ppermute | solution.py:31
  57.9 1.9 %collective-permute-start.2 = (f32[128,128]{1,0:T(8,128)S(1)}, f32[128,128]{1,0:T(8,128)S(1)}, u32[]{:S(2)}, u32[]{:S(2)}) collective-permute-start(f32[128,128]{1,0:T(8,128)S(1)} %constant_dynamic-slice_fusion), channel_id=1, source_target_pairs={{0,4},{4,0},{1,5},{5,1},{2,6},{6,2},{3,7},{7,3},{8,12},{12,8},{9,1... | collective-permute-start | bytes 196616 | tf_op jit(solution)/shard_map/ppermute | solution.py:31
  59.9 2.2 %collective-permute-start.1 = (bf16[16,2048]{1,0:T(8,128)(2,1)S(1)}, bf16[16,2048]{1,0:T(8,128)(2,1)S(1)}, u32[]{:S(2)}, u32[]{:S(2)}) collective-permute-start(bf16[16,2048]{1,0:T(8,128)(2,1)S(1)} %bitcast.34), channel_id=1, source_target_pairs={{0,4},{4,8},{8,12},{12,16},{16,20},{20,24},{24,28},{28,32},{32,36}... | collective-permute-start | bytes 196616 | tf_op jit(solution)/shard_map/ppermute | solution.py:36
  62.1 1.3 collective-permute-done.1.halo
  63.4 5.0 %all-gather.5.cloned.1.call-done.weights = bf16[2048,512]{1,0:T(8,128)(2,1)} async-done(((bf16[128,512]{1,0:T(8,128)(2,1)}), bf16[2048,512]{1,0:T(8,128)(2,1)}) %all-gather.5.cloned.1.call-update) | async-done | bytes 2097168 | tf_op jit(solution)/shard_map/all_gather | solution.py:295
  68.5 3.5 %chip_state.1 = (bf16[8,144,128]{2,1,0:T(8,128)(2,1)}, f32[9,128,128]{2,1,0:T(8,128)S(1)}) custom-call(s32[1]{0:T(128)} %bitcast.3.core, bf16[128,2048]{1,0:T(8,128)(2,1)S(1)} %bitcast.25, bf16[128,2048]{1,0:T(8,128)(2,1)S(1)} %collective-permute-done.partner, bf16[2048,512]{1,0:T(8,128)(2,1)} %all-gather.5.cloned.1.call-done.weights, ...), custom_call_target="tpu_custom_call" | custom-call | tf_op jit(solution)/shard_map/chip_state/pallas_call | solution.py:329
  72.0 6.5 %all-to-all-start.3 = ((bf16[8,144,128]{2,1,0:T(8,128)(2,1)}), bf16[8,144,128]{2,1,0:T(8,128)(2,1)S(1)}, u32[]{:S(2)}, u32[]{:S(2)}) async-start(bf16[8,144,128]{2,1,0:T(8,128)(2,1)} %get-tuple-element.21), calls=%async_computation.3 | async-start | bytes 589824 | tf_op jit(solution)/shard_map/all_to_all | solution.py:23
  78.5 12.9 %all-to-all-done.3.arrived = bf16[8,144,128]{2,1,0:T(8,128)(2,1)S(1)} async-done(((bf16[8,144,128]{2,1,0:T(8,128)(2,1)}), bf16[8,144,128]{2,1,0:T(8,128)(2,1)S(1)}, u32[]{:S(2)}, u32[]{:S(2)}) %all-to-all-start.3) | async-done | bytes 294944 | tf_op jit(solution)/shard_map/all_to_all | solution.py:23
  91.4 0.8 along_row.1
  92.2 3.6 %all-to-all-start.4 = ((bf16[8,144,128]{2,1,0:T(8,128)(2,1)}), bf16[8,144,128]{2,1,0:T(8,128)(2,1)S(1)}, u32[]{:S(2)}, u32[]{:S(2)}) async-start(bf16[8,144,128]{2,1,0:T(8,128)(2,1)} %get-tuple-element.22), calls=%async_computation.4 | async-start | bytes 589824 | tf_op jit(solution)/shard_map/all_to_all | solution.py:23
  95.8 14.8 %all-to-all-done.4.arrived = bf16[8,144,128]{2,1,0:T(8,128)(2,1)S(1)} async-done(((bf16[8,144,128]{2,1,0:T(8,128)(2,1)}), bf16[8,144,128]{2,1,0:T(8,128)(2,1)S(1)}, u32[]{:S(2)}, u32[]{:S(2)}) %all-to-all-start.4) | async-done | bytes 294944 | tf_op jit(solution)/shard_map/all_to_all | solution.py:23
  110.7 5.6 %all_to_all.36.incoming = bf16[2,128,128]{2,1,0:T(8,128)(2,1)S(1)} all-to-all(bf16[2,128,128]{2,1,0:T(8,128)(2,1)S(1)} %enter_chip.1), channel_id=1, replica_groups=mesh['sp_0'=8,'sp_1'=8,'sp_2'=2,'tp'=4] {'sp_2'}, dimensions={0} | all-to-all | bytes 131072 | tf_op jit(solution)/shard_map/all_to_all | solution.py:23
  116.3 2.2 %all-gather.3.cloned.1.call-done.weights = bf16[2048,1024]{1,0:T(8,128)(2,1)} async-done(((bf16[128,1024]{1,0:T(8,128)(2,1)}), bf16[2048,1024]{1,0:T(8,128)(2,1)}) %all-gather.3.cloned.1.call-update) | async-done | bytes 4194320 | tf_op jit(solution)/shard_map/all_gather | solution.py:297
  118.4 4.6 %outputs.1 = bf16[128,2048]{1,0:T(8,128)(2,1)S(1)} custom-call(bf16[16,2048]{1,0:T(8,128)(2,1)} %copy-done.8, bf16[128,2048]{1,0:T(8,128)(2,1)} %bitcast.26, bf16[2048,1024]{1,0:T(8,128)(2,1)} %all-gather.3.cloned.1.call-done.weights, f32[9,128,128]{2,1,0:T(8,128)S(1)} %get-tuple-element.20.carried, f32[3,256]{1,0:T(4,128)S(1)} %copy-done.2, ...), custom_call_target="tpu_custom_call" | custom-call | tf_op jit(solution)/shard_map/outputs/pallas_call | solution.py:372
  123.0 13.0 %all_to_all.37 = bf16[4,32,2048]{2,1,0:T(8,128)(2,1)S(1)} all-to-all(bf16[4,32,2048]{2,1,0:T(8,128)(2,1)S(1)} %bitcast.27), channel_id=1, replica_groups=mesh['sp_0'=8,'sp_1'=8,'sp_2'=2,'tp'=4] {'tp'}, dimensions={0} | all-to-all | bytes 1048576 | tf_op jit(solution)/shard_map/all_to_all | solution.py:23
  136.0 0.7 reduce_sum.22
  (38 shorter events, 3.3 us)
Async XLA Ops:
  6.5 43.6 %copy-start.6 = (bf16[256,256,1]{1,0,2:T(8,128)(2,1)S(1)}, bf16[256,256,1]{1,0,2:T(8,128)(2,1)}, u32[]{:S(2)}) copy-start(bf16[256,256,1]{1,0,2:T(8,128)(2,1)} %constant.43) | copy-start | bytes 393220
  8.0 15.7 %all-to-all-start.1 = ((bf16[8,16,512]{2,1,0:T(8,128)(2,1)}), bf16[8,16,512]{2,1,0:T(8,128)(2,1)S(1)}, u32[]{:S(2)}, u32[]{:S(2)}) async-start(bf16[8,16,512]{2,1,0:T(8,128)(2,1)} %broadcast_in_dim.18), calls=%async_computation.1 | async-start | bytes 262144 | tf_op jit(solution)/shard_map/all_to_all | solution.py:23
  15.6 52.9 %all-gather.5.cloned.1.call-start = ((), (), s32[]{:S(2)}) async-start(), calls=%async_computation.8 | async-start | bytes 2228224 | tf_op jit(solution)/shard_map/all_gather | solution.py:295
  23.6 0.7 copy-start.5
  24.3 94.1 %all-gather.3.cloned.1.call-start = ((), (), s32[]{:S(2)}) async-start(), calls=%async_computation.7 | async-start | bytes 4456448 | tf_op jit(solution)/shard_map/all_gather | solution.py:297
  24.4 33.5 %copy-start.1 = (f32[128,256]{1,0:T(8,128)S(1)}, f32[128,256]{1,0:T(8,128)}, u32[]{:S(2)}) copy-start(f32[128,256]{1,0:T(8,128)} %fade.1) | copy-start | bytes 393220
  37.1 31.4 %copy-start.3 = (f32[256]{0:T(256)S(1)}, f32[256]{0:T(256)}, u32[]{:S(2)}) copy-start(f32[256]{0:T(256)} %param.25) | copy-start | bytes 3076
  38.9 10.6 %all-to-all-start = ((bf16[4,32,2048]{2,1,0:T(8,128)(2,1)}), bf16[4,32,2048]{2,1,0:T(8,128)(2,1)S(1)}, u32[]{:S(2)}, u32[]{:S(2)}) async-start(bf16[4,32,2048]{2,1,0:T(8,128)(2,1)} %broadcast_in_dim.17), calls=%async_computation | async-start | bytes 1048576 | tf_op jit(solution)/shard_map/all_to_all | solution.py:23
  50.5 67.9 %copy-start.2 = (f32[3,256]{1,0:T(4,128)S(1)}, f32[3,256]{1,0:T(4,128)}, u32[]{:S(2)}) copy-start(f32[3,256]{1,0:T(4,128)} %taps.1) | copy-start | bytes 9220
  50.5 67.9 %copy-start.4 = (f32[128]{0:T(128)S(1)}, f32[128]{0:T(128)}, u32[]{:S(2)}) copy-start(f32[128]{0:T(128)} %param.27) | copy-start | bytes 1540
  50.6 67.9 %copy-start = (bf16[8,16,8,256]{3,2,0,1:T(8,128)(2,1)}, bf16[8,16,8,256]{3,2,0,1:T(8,128)(2,1)S(1)}, u32[]{:S(2)}) copy-start(bf16[8,16,8,256]{3,2,0,1:T(8,128)(2,1)S(1)} %copy.22) | copy-start | bytes 1572868
  50.6 12.9 %collective-permute-start = (bf16[128,2048]{1,0:T(8,128)(2,1)S(1)}, bf16[128,2048]{1,0:T(8,128)(2,1)S(1)}, u32[]{:S(2)}, u32[]{:S(2)}) collective-permute-start(bf16[128,2048]{1,0:T(8,128)(2,1)S(1)} %bitcast.24), channel_id=1, source_target_pairs={{0,4},{4,0},{1,5},{5,1},{2,6},{6,2},{3,7},{7,3},{8,12},{12,8},{9,1... | collective-permute-start | bytes 1572872 | tf_op jit(solution)/shard_map/ppermute | solution.py:31
  57.9 4.2 %collective-permute-start.2 = (f32[128,128]{1,0:T(8,128)S(1)}, f32[128,128]{1,0:T(8,128)S(1)}, u32[]{:S(2)}, u32[]{:S(2)}) collective-permute-start(f32[128,128]{1,0:T(8,128)S(1)} %constant_dynamic-slice_fusion), channel_id=1, source_target_pairs={{0,4},{4,0},{1,5},{5,1},{2,6},{6,2},{3,7},{7,3},{8,12},{12,8},{9,1... | collective-permute-start | bytes 196616 | tf_op jit(solution)/shard_map/ppermute | solution.py:31
  59.9 3.5 %collective-permute-start.1 = (bf16[16,2048]{1,0:T(8,128)(2,1)S(1)}, bf16[16,2048]{1,0:T(8,128)(2,1)S(1)}, u32[]{:S(2)}, u32[]{:S(2)}) collective-permute-start(bf16[16,2048]{1,0:T(8,128)(2,1)S(1)} %bitcast.34), channel_id=1, source_target_pairs={{0,4},{4,8},{8,12},{12,16},{16,20},{20,24},{24,28},{28,32},{32,36}... | collective-permute-start | bytes 196616 | tf_op jit(solution)/shard_map/ppermute | solution.py:36
  62.1 6.4 %copy-start.7 = (f32[128,128]{1,0:T(8,128)}, f32[128,128]{1,0:T(8,128)S(1)}, u32[]{:S(2)}) copy-start(f32[128,128]{1,0:T(8,128)S(1)} %collective-permute-done.2.partner_fade) | copy-start | bytes 196612
  63.4 55.0 %copy-start.8 = (bf16[16,2048]{1,0:T(8,128)(2,1)}, bf16[16,2048]{1,0:T(8,128)(2,1)S(1)}, u32[]{:S(2)}) copy-start(bf16[16,2048]{1,0:T(8,128)(2,1)S(1)} %collective-permute-done.1.halo) | copy-start | bytes 196612
  72.0 19.4 %all-to-all-start.3 = ((bf16[8,144,128]{2,1,0:T(8,128)(2,1)}), bf16[8,144,128]{2,1,0:T(8,128)(2,1)S(1)}, u32[]{:S(2)}, u32[]{:S(2)}) async-start(bf16[8,144,128]{2,1,0:T(8,128)(2,1)} %get-tuple-element.21), calls=%async_computation.3 | async-start | bytes 589824 | tf_op jit(solution)/shard_map/all_to_all | solution.py:23
  92.2 18.4 %all-to-all-start.4 = ((bf16[8,144,128]{2,1,0:T(8,128)(2,1)}), bf16[8,144,128]{2,1,0:T(8,128)(2,1)S(1)}, u32[]{:S(2)}, u32[]{:S(2)}) async-start(bf16[8,144,128]{2,1,0:T(8,128)(2,1)} %get-tuple-element.22), calls=%async_computation.4 | async-start | bytes 589824 | tf_op jit(solution)/shard_map/all_to_all | solution.py:23
Sparse Core Ops, SparseCore 0:
  24.4 44.0 all-gather.4
  70.6 47.7 all-gather.2

commit v4 on v3

--- a/solution.py
+++ b/solution.py
@@ -71,7 +71,7 @@
 
 
 def state_kernel(
-    core, own, partner, weights, gap, fade, partner_fade, initial,
+    places, own, partner, weights, gap, fade, partner_fade, initial,
     packed, carried,
     held, fade_held, initial_held, sems, small_sems,
 ):
@@ -83,7 +83,7 @@
     ]
     small_copies = [
         pltpu.make_async_copy(partner_fade, fade_held, small_sems.at[0]),
-        pltpu.make_async_copy(initial.at[core[0]], initial_held, small_sems.at[1]),
+        pltpu.make_async_copy(initial.at[places[2]], initial_held, small_sems.at[1]),
     ]
     for copy in copies + small_copies:
         copy.start()
@@ -97,7 +97,7 @@
     for copy in small_copies:
         copy.wait()
     logits = total.astype(bf16).astype(f32)
-    first = core[0] == 0
+    first = places[2] == 0
 
     def head(a):
         return jnp.where(first, a[:, :HEAD_DIM], a[:, HEAD_DIM:])
@@ -152,12 +152,12 @@
     return decay, state
 
 
-def row_kernel(place, arrived, carried, packed, decays, states):
+def row_kernel(places, arrived, carried, packed, decays, states):
     decay, state = before_place(arrived, arrived.shape[0])
     out = packed_rows(decay, state)
     for k in range(packed.shape[0]):
         packed[k] = out
-    decay, state = before_place(arrived, place[0])
+    decay, state = before_place(arrived, places[1])
     decay_0 = carried[DECAY_0, 0:1]
     decays[0:1] = decay
     decays[1:2] = decay + decay_0
@@ -165,8 +165,8 @@
     states[1] = jnp.exp(decay_0) * state + carried[STATE_0]
 
 
-def enter_kernel(place, arrived, carried, decays, states, incoming):
-    decay, state = before_place(arrived, place[0])
+def enter_kernel(places, arrived, carried, decays, states, incoming):
+    decay, state = before_place(arrived, places[0])
     before = jnp.exp(decay) * carried[INITIAL] + state
     for k in range(2):
         incoming[k] = (jnp.exp(decays[k : k + 1]) * before + states[k]).astype(bf16)
@@ -175,7 +175,7 @@
 def final_kernel(
     halo, own, weights, carried, taps, incoming, head_gain, w_filter, w_rec,
     partial,
-    held, rows, out_filter, out_rec, sems, row_sems, out_sems,
+    held, rows, out_rec, sems, row_sems, out_sems,
 ):
     length = own.shape[0]
     piece = weights.shape[0] // PIECES
@@ -184,8 +184,7 @@
         pltpu.make_async_copy(own, rows.at[pl.ds(HALO, length)], row_sems.at[1]),
     ]
     out_copies = [
-        pltpu.make_async_copy(w_filter, out_filter, out_sems.at[0]),
-        pltpu.make_async_copy(w_rec, out_rec, out_sems.at[1]),
+        pltpu.make_async_copy(w_rec, out_rec, out_sems.at[0]),
     ]
     for copy in row_copies:
         copy.start()
@@ -249,7 +248,7 @@
     for copy in out_copies:
         copy.wait()
     partial[...] = (
-        jnp.dot(filter_out, out_filter[...], preferred_element_type=f32)
+        jnp.dot(filter_out, w_filter[...], preferred_element_type=f32)
         + jnp.dot(rec_out, out_rec[...], preferred_element_type=f32)
     ).astype(bf16)
 
@@ -320,9 +319,11 @@
     head = lambda a, k: lax.dynamic_slice_in_dim(a, k * HEAD_DIM, HEAD_DIM, axis=1)
     partner_fade = swapped(head(fade, 1 - c), "sp_2")
 
-    partner, halo, partner_fade = lax.optimization_barrier((partner, halo, partner_fade))
-
-    core = jnp.stack([c])
+    places = jnp.stack([z, y, c])
+    partner, halo, partner_fade, places = lax.optimization_barrier(
+        (partner, halo, partner_fade, places)
+    )
+
     dma = pltpu.SemaphoreType.DMA
     square = (HEAD_DIM, HEAD_DIM)
     packed_shape = jax.ShapeDtypeStruct((8, HEAD_DIM + 16, HEAD_DIM), bf16)
@@ -341,7 +342,7 @@
         name="chip_state",
         compiler_params=granted(12),
     )(
-        core,
+        places,
         near(own),
         near(partner),
         far(state_weights),
@@ -358,7 +359,7 @@
         out_shape=[packed_shape, made((8, HEAD_DIM), f32), made((2, *square), f32)],
         name="along_row",
         compiler_params=granted(4),
-    )(jnp.stack([y]), near(exchanged(packed, "sp_1")), carried)
+    )(places, near(exchanged(packed, "sp_1")), carried)
     incoming = pl.pallas_call(
         enter_kernel,
         in_specs=[SMEM] + [VMEM] * 4,
@@ -366,22 +367,21 @@
         out_shape=made((2, *square), bf16),
         name="enter_chip",
         compiler_params=granted(4),
-    )(jnp.stack([z]), near(exchanged(packed, "sp_0")), carried, decays, states)
+    )(places, near(exchanged(packed, "sp_0")), carried, decays, states)
     incoming = exchanged(incoming, "sp_2")
 
     partial = pl.pallas_call(
         final_kernel,
-        in_specs=[ANY, ANY, ANY] + [VMEM] * 4 + [ANY, ANY],
+        in_specs=[ANY, ANY, ANY] + [VMEM] * 5 + [ANY],
         out_specs=VMEM,
         out_shape=made((length, width), bf16),
         scratch_shapes=[
             pltpu.VMEM((PIECES, width // PIECES, 1024), bf16),
             pltpu.VMEM((HALO + length, width), bf16),
             pltpu.VMEM((256, width), bf16),
-            pltpu.VMEM((256, width), bf16),
             dma((PIECES,)),
             dma((2,)),
-            dma((2,)),
+            dma((1,)),
         ],
         name="outputs",
         compiler_params=granted(20),
@@ -393,7 +393,7 @@
         near(filter_taps),
         near(incoming),
         near(head_gain[None]),
-        far(w_out_filter),
+        near(w_out_filter),
         far(w_out_rec),
     )
     arrived = exchanged(partial.reshape(4, length // 4, -1), "tp")

time: 144 us -> 144 us (level)
  blocking collectives: 31.3 us -> 68.4 us
  waiting for transfers between devices: 49.7 us -> 22.4 us
  starting transfers between devices: 32.9 us -> 23 us
    all_to_all x3 -> x5, blocking collectives: 31.3 us -> 68.4 us  [exchanged(): return lax.all_to_all(blocks, axis, split_axis=0, concat_axis=0, tiled=True)]
    all_to_all x4 -> x2, waiting for transfers between devices: 41.2 us -> 13.5 us  [exchanged(): return lax.all_to_all(blocks, axis, split_axis=0, concat_axis=0, tiled=True)]
    all_to_all x4 -> x2, starting transfers between devices: 21.4 us -> 11.3 us  [exchanged(): return lax.all_to_all(blocks, axis, split_axis=0, concat_axis=0, tiled=True)]
  transfers between devices with their start and end apart: 9 -> 7, of which waited for: 7 -> 5; matrix products, arithmetic and copies ran while one was open for 3% -> 3% of each run, Pallas kernels for 3% -> 3%
where the time goes in v4:
time: 144 us; the launch traced here: 143 us
  blocking collectives  68.4 us (48%)
  starting transfers between devices  23 us (16%)
  waiting for transfers between devices  22.4 us (16%)
  between operations  13.6 us (9%)
  Pallas kernels  8.85 us (6%)
  local copies, waits for them, and re-layouts  4.1 us (3%)
  other arithmetic  2.73 us (2%)
    all_to_all x5, blocking collectives, exchanged(): return lax.all_to_all(blocks, axis, split_axis=0, concat_axis=0, tiled=True)  68.4 us
    all_to_all x2, waiting for transfers between devices, exchanged(): return lax.all_to_all(blocks, axis, split_axis=0, concat_axis=0, tiled=True)  13.5 us
    all_to_all x2, starting transfers between devices, exchanged(): return lax.all_to_all(blocks, axis, split_axis=0, concat_axis=0, tiled=True)  11.3 us
    ppermute x2, starting transfers between devices, swapped(): return lax.ppermute(x, axis, [(0, 1), (1, 0)])  9.36 us
    all_gather x1, waiting for transfers between devices, body(): lax.all_gather(state_along_y, ('sp_0', 'sp_2'), axis=0, tiled=True)  4.9 us
    pallas_call x1, Pallas kernels, body(): pl.pallas_call(final_kernel, in_specs=[ANY, ANY, ANY] + [VMEM] * 5 + [ANY...  4.23 us
    pallas_call x1, Pallas kernels, body(): pl.pallas_call(state_kernel, in_specs=[SMEM, VMEM, VMEM, ANY, VMEM, VMEM,...  3.32 us
  transfers between devices with their start and end apart: 7, of which 5 were waited for; matrix products, arithmetic and copies ran while one was open for 3% of the time, Pallas kernels for 3%

profile of v4, /device:TPU:1, one launch (start us, length us, event | category | flops | bytes accessed | tf_op | source)
XLA Modules:
  0.0 143.4 jit_solution(8814951878010756955)
XLA Ops:
  6.5 0.8 pad_maximum_fusion.1
  7.3 0.7 broadcast_in_dim.18
  8.0 7.6 %all-to-all-start.1 = ((bf16[8,16,512]{2,1,0:T(8,128)(2,1)}), bf16[8,16,512]{2,1,0:T(8,128)(2,1)S(1)}, u32[]{:S(2)}, u32[]{:S(2)}) async-start(bf16[8,16,512]{2,1,0:T(8,128)(2,1)} %broadcast_in_dim.18), calls=%async_computation.1 | async-start | bytes 262144 | tf_op jit(solution)/shard_map/all_to_all | solution.py:23
  15.6 0.8 pad_maximum_fusion
  16.4 7.2 %all-to-all-done.1 = bf16[8,16,512]{2,1,0:T(8,128)(2,1)S(1)} async-done(((bf16[8,16,512]{2,1,0:T(8,128)(2,1)}), bf16[8,16,512]{2,1,0:T(8,128)(2,1)S(1)}, u32[]{:S(2)}, u32[]{:S(2)}) %all-to-all-start.1) | async-done | bytes 131104 | tf_op jit(solution)/shard_map/all_to_all | solution.py:23
  24.4 12.7 %all_to_all.35 = bf16[8,16,1024]{2,1,0:T(8,128)(2,1)} all-to-all(bf16[8,16,1024]{2,1,0:T(8,128)(2,1)S(1)} %broadcast_in_dim.19), channel_id=1, replica_groups=mesh['sp_0'=8,'sp_1'=8,'sp_2'=2,'tp'=4] {'sp_1'}, dimensions={0} | all-to-all | bytes 524288 | tf_op jit(solution)/shard_map/all_to_all | solution.py:23
  37.1 1.8 %broadcast_in_dim.17 = bf16[4,32,2048]{2,1,0:T(8,128)(2,1)} broadcast(bf16[32,2048]{1,0:T(8,128)(2,1)} %param.16), dimensions={1,2} | broadcast | bytes 655360 | tf_op jit(solution)/shard_map/broadcast_in_dim | solution.py:27
  38.9 3.7 %all-to-all-start = ((bf16[4,32,2048]{2,1,0:T(8,128)(2,1)}), bf16[4,32,2048]{2,1,0:T(8,128)(2,1)S(1)}, u32[]{:S(2)}, u32[]{:S(2)}) async-start(bf16[4,32,2048]{2,1,0:T(8,128)(2,1)} %broadcast_in_dim.17), calls=%async_computation | async-start | bytes 1048576 | tf_op jit(solution)/shard_map/all_to_all | solution.py:23
  42.6 0.7 mul.30
  43.3 6.2 %all-to-all-done = bf16[4,32,2048]{2,1,0:T(8,128)(2,1)S(1)} async-done(((bf16[4,32,2048]{2,1,0:T(8,128)(2,1)}), bf16[4,32,2048]{2,1,0:T(8,128)(2,1)S(1)}, u32[]{:S(2)}, u32[]{:S(2)}) %all-to-all-start) | async-done | bytes 524320 | tf_op jit(solution)/shard_map/all_to_all | solution.py:23
  50.6 7.4 %collective-permute-start = (bf16[128,2048]{1,0:T(8,128)(2,1)S(1)}, bf16[128,2048]{1,0:T(8,128)(2,1)S(1)}, u32[]{:S(2)}, u32[]{:S(2)}) collective-permute-start(bf16[128,2048]{1,0:T(8,128)(2,1)S(1)} %bitcast.24), channel_id=1, source_target_pairs={{0,4},{4,0},{1,5},{5,1},{2,6},{6,2},{3,7},{7,3},{8,12},{12,8},{9,1... | collective-permute-start | bytes 1572872 | tf_op jit(solution)/shard_map/ppermute | solution.py:31
  58.1 1.9 %collective-permute-start.2 = (f32[128,128]{1,0:T(8,128)S(1)}, f32[128,128]{1,0:T(8,128)S(1)}, u32[]{:S(2)}, u32[]{:S(2)}) collective-permute-start(f32[128,128]{1,0:T(8,128)S(1)} %constant_dynamic-slice_fusion), channel_id=1, source_target_pairs={{0,4},{4,0},{1,5},{5,1},{2,6},{6,2},{3,7},{7,3},{8,12},{12,8},{9,1... | collective-permute-start | bytes 196616 | tf_op jit(solution)/shard_map/ppermute | solution.py:31
  60.0 2.2 %collective-permute-start.1 = (bf16[16,2048]{1,0:T(8,128)(2,1)S(1)}, bf16[16,2048]{1,0:T(8,128)(2,1)S(1)}, u32[]{:S(2)}, u32[]{:S(2)}) collective-permute-start(bf16[16,2048]{1,0:T(8,128)(2,1)S(1)} %bitcast.34), channel_id=1, source_target_pairs={{0,4},{4,8},{8,12},{12,16},{16,20},{20,24},{24,28},{28,32},{32,36}... | collective-permute-start | bytes 196616 | tf_op jit(solution)/shard_map/ppermute | solution.py:36
  62.3 1.2 collective-permute-done.1.halo
  63.6 4.9 %all-gather.5.cloned.1.call-done.weights = bf16[2048,512]{1,0:T(8,128)(2,1)} async-done(((bf16[128,512]{1,0:T(8,128)(2,1)}), bf16[2048,512]{1,0:T(8,128)(2,1)}) %all-gather.5.cloned.1.call-update) | async-done | bytes 2097168 | tf_op jit(solution)/shard_map/all_gather | solution.py:294
  68.5 3.3 %chip_state.1 = (bf16[8,144,128]{2,1,0:T(8,128)(2,1)S(1)}, f32[9,128,128]{2,1,0:T(8,128)S(1)}) custom-call(s32[3]{0:T(128)S(1)} %pad_add_fusion.places, bf16[128,2048]{1,0:T(8,128)(2,1)S(1)} %bitcast.25, bf16[128,2048]{1,0:T(8,128)(2,1)S(1)} %collective-permute-done.partner, bf16[2048,512]{1,0:T(8,128)(2,1)} %all-gather.5.cloned.1.call-done.weights, ...), custom_call_target="tpu_custom_call" | custom-call | tf_op jit(solution)/shard_map/chip_state/pallas_call | solution.py:330
  71.8 18.6 %all_to_all.36.arrived = bf16[8,144,128]{2,1,0:T(8,128)(2,1)S(1)} all-to-all(bf16[8,144,128]{2,1,0:T(8,128)(2,1)S(1)} %get-tuple-element.23), channel_id=1, replica_groups=mesh['sp_0'=8,'sp_1'=8,'sp_2'=2,'tp'=4] {'sp_1'}, dimensions={0} | all-to-all | bytes 589824 | tf_op jit(solution)/shard_map/all_to_all | solution.py:23
  90.4 0.7 along_row.1
  91.1 18.3 %all_to_all.37.arrived = bf16[8,144,128]{2,1,0:T(8,128)(2,1)S(1)} all-to-all(bf16[8,144,128]{2,1,0:T(8,128)(2,1)S(1)} %get-tuple-element.24), channel_id=1, replica_groups=mesh['sp_0'=8,'sp_1'=8,'sp_2'=2,'tp'=4] {'sp_0'}, dimensions={0} | all-to-all | bytes 589824 | tf_op jit(solution)/shard_map/all_to_all | solution.py:23
  110.1 6.0 %all_to_all.38.incoming = bf16[2,128,128]{2,1,0:T(8,128)(2,1)S(1)} all-to-all(bf16[2,128,128]{2,1,0:T(8,128)(2,1)S(1)} %enter_chip.1), channel_id=1, replica_groups=mesh['sp_0'=8,'sp_1'=8,'sp_2'=2,'tp'=4] {'sp_2'}, dimensions={0} | all-to-all | bytes 131072 | tf_op jit(solution)/shard_map/all_to_all | solution.py:23
  116.0 2.8 %all-gather.3.cloned.1.call-done.weights = bf16[2048,1024]{1,0:T(8,128)(2,1)} async-done(((bf16[128,1024]{1,0:T(8,128)(2,1)}), bf16[2048,1024]{1,0:T(8,128)(2,1)}) %all-gather.3.cloned.1.call-update) | async-done | bytes 4194320 | tf_op jit(solution)/shard_map/all_gather | solution.py:296
  118.8 4.2 %outputs.1 = bf16[128,2048]{1,0:T(8,128)(2,1)S(1)} custom-call(bf16[16,2048]{1,0:T(8,128)(2,1)} %copy-done.9, bf16[128,2048]{1,0:T(8,128)(2,1)} %bitcast.26, bf16[2048,1024]{1,0:T(8,128)(2,1)} %all-gather.3.cloned.1.call-done.weights, f32[9,128,128]{2,1,0:T(8,128)S(1)} %get-tuple-element.22.carried, f32[3,256]{1,0:T(4,128)S(1)} %copy-done.3, ...), custom_call_target="tpu_custom_call" | custom-call | tf_op jit(solution)/shard_map/outputs/pallas_call | solution.py:373
  123.1 12.8 %all_to_all.39 = bf16[4,32,2048]{2,1,0:T(8,128)(2,1)S(1)} all-to-all(bf16[4,32,2048]{2,1,0:T(8,128)(2,1)S(1)} %bitcast.27), channel_id=1, replica_groups=mesh['sp_0'=8,'sp_1'=8,'sp_2'=2,'tp'=4] {'tp'}, dimensions={0} | all-to-all | bytes 1048576 | tf_op jit(solution)/shard_map/all_to_all | solution.py:23
  135.8 0.7 reduce_sum.22
  (39 shorter events, 2.5 us)
Async XLA Ops:
  6.5 43.6 %copy-start.7 = (bf16[256,256,1]{1,0,2:T(8,128)(2,1)S(1)}, bf16[256,256,1]{1,0,2:T(8,128)(2,1)}, u32[]{:S(2)}) copy-start(bf16[256,256,1]{1,0,2:T(8,128)(2,1)} %constant.43) | copy-start | bytes 393220
  8.0 15.7 %all-to-all-start.1 = ((bf16[8,16,512]{2,1,0:T(8,128)(2,1)}), bf16[8,16,512]{2,1,0:T(8,128)(2,1)S(1)}, u32[]{:S(2)}, u32[]{:S(2)}) async-start(bf16[8,16,512]{2,1,0:T(8,128)(2,1)} %broadcast_in_dim.18), calls=%async_computation.1 | async-start | bytes 262144 | tf_op jit(solution)/shard_map/all_to_all | solution.py:23
  15.6 52.9 %all-gather.5.cloned.1.call-start = ((), (), s32[]{:S(2)}) async-start(), calls=%async_computation.8 | async-start | bytes 2228224 | tf_op jit(solution)/shard_map/all_gather | solution.py:294
  23.6 0.7 copy-start.6
  24.3 94.5 %all-gather.3.cloned.1.call-start = ((), (), s32[]{:S(2)}) async-start(), calls=%async_computation.7 | async-start | bytes 4456448 | tf_op jit(solution)/shard_map/all_gather | solution.py:296
  24.4 33.6 %copy-start.2 = (f32[128,256]{1,0:T(8,128)S(1)}, f32[128,256]{1,0:T(8,128)}, u32[]{:S(2)}) copy-start(f32[128,256]{1,0:T(8,128)} %fade.1) | copy-start | bytes 393220
  37.1 31.4 %copy-start.4 = (f32[256]{0:T(256)S(1)}, f32[256]{0:T(256)}, u32[]{:S(2)}) copy-start(f32[256]{0:T(256)} %param.25) | copy-start | bytes 3076
  38.9 10.6 %all-to-all-start = ((bf16[4,32,2048]{2,1,0:T(8,128)(2,1)}), bf16[4,32,2048]{2,1,0:T(8,128)(2,1)S(1)}, u32[]{:S(2)}, u32[]{:S(2)}) async-start(bf16[4,32,2048]{2,1,0:T(8,128)(2,1)} %broadcast_in_dim.17), calls=%async_computation | async-start | bytes 1048576 | tf_op jit(solution)/shard_map/all_to_all | solution.py:23
  50.5 68.3 %copy-start.1 = (bf16[256,2048]{1,0:T(8,128)(2,1)S(1)}, bf16[256,2048]{1,0:T(8,128)(2,1)}, u32[]{:S(2)}) copy-start(bf16[256,2048]{1,0:T(8,128)(2,1)} %w_filter.1) | copy-start | bytes 3145732
  50.5 68.3 %copy-start.3 = (f32[3,256]{1,0:T(4,128)S(1)}, f32[3,256]{1,0:T(4,128)}, u32[]{:S(2)}) copy-start(f32[3,256]{1,0:T(4,128)} %taps.1) | copy-start | bytes 9220
  50.5 68.3 %copy-start.5 = (f32[128]{0:T(128)S(1)}, f32[128]{0:T(128)}, u32[]{:S(2)}) copy-start(f32[128]{0:T(128)} %param.27) | copy-start | bytes 1540
  50.6 68.2 %copy-start = (bf16[8,16,8,256]{3,2,0,1:T(8,128)(2,1)}, bf16[8,16,8,256]{3,2,0,1:T(8,128)(2,1)S(1)}, u32[]{:S(2)}) copy-start(bf16[8,16,8,256]{3,2,0,1:T(8,128)(2,1)S(1)} %copy.22) | copy-start | bytes 1572868
  50.6 13.0 %collective-permute-start = (bf16[128,2048]{1,0:T(8,128)(2,1)S(1)}, bf16[128,2048]{1,0:T(8,128)(2,1)S(1)}, u32[]{:S(2)}, u32[]{:S(2)}) collective-permute-start(bf16[128,2048]{1,0:T(8,128)(2,1)S(1)} %bitcast.24), channel_id=1, source_target_pairs={{0,4},{4,0},{1,5},{5,1},{2,6},{6,2},{3,7},{7,3},{8,12},{12,8},{9,1... | collective-permute-start | bytes 1572872 | tf_op jit(solution)/shard_map/ppermute | solution.py:31
  58.1 4.3 %collective-permute-start.2 = (f32[128,128]{1,0:T(8,128)S(1)}, f32[128,128]{1,0:T(8,128)S(1)}, u32[]{:S(2)}, u32[]{:S(2)}) collective-permute-start(f32[128,128]{1,0:T(8,128)S(1)} %constant_dynamic-slice_fusion), channel_id=1, source_target_pairs={{0,4},{4,0},{1,5},{5,1},{2,6},{6,2},{3,7},{7,3},{8,12},{12,8},{9,1... | collective-permute-start | bytes 196616 | tf_op jit(solution)/shard_map/ppermute | solution.py:31
  60.0 3.6 %collective-permute-start.1 = (bf16[16,2048]{1,0:T(8,128)(2,1)S(1)}, bf16[16,2048]{1,0:T(8,128)(2,1)S(1)}, u32[]{:S(2)}, u32[]{:S(2)}) collective-permute-start(bf16[16,2048]{1,0:T(8,128)(2,1)S(1)} %bitcast.34), channel_id=1, source_target_pairs={{0,4},{4,8},{8,12},{12,16},{16,20},{20,24},{24,28},{28,32},{32,36}... | collective-permute-start | bytes 196616 | tf_op jit(solution)/shard_map/ppermute | solution.py:36
  62.3 6.1 %copy-start.8 = (f32[128,128]{1,0:T(8,128)}, f32[128,128]{1,0:T(8,128)S(1)}, u32[]{:S(2)}) copy-start(f32[128,128]{1,0:T(8,128)S(1)} %collective-permute-done.2.partner_fade) | copy-start | bytes 196612
  63.6 55.2 %copy-start.9 = (bf16[16,2048]{1,0:T(8,128)(2,1)}, bf16[16,2048]{1,0:T(8,128)(2,1)S(1)}, u32[]{:S(2)}) copy-start(bf16[16,2048]{1,0:T(8,128)(2,1)S(1)} %collective-permute-done.1.halo) | copy-start | bytes 196612
Sparse Core Ops, SparseCore 0:
  24.4 44.0 all-gather.4
  70.6 48.1 all-gather.2

commit v5 on v4

--- a/solution.py
+++ b/solution.py
@@ -40,7 +40,7 @@
 ANY = pl.BlockSpec(memory_space=pl.ANY)
 VMEM = pl.BlockSpec(memory_space=pltpu.VMEM)
 SMEM = pl.BlockSpec(memory_space=pltpu.SMEM)
-PIECES = 4
+PIECES = 2
 RATE, RUNNING, VALUE, STATE_0, INITIAL, DECAY_0, CARRIED = 0, 2, 4, 6, 7, 8, 9
 
 

time: 144 us -> 144 us (level)
  no operation moved by 1% of the time
where the time goes in v5:
time: 144 us
  blocking collectives  68.5 us (48%)
  starting transfers between devices  23 us (16%)
  waiting for transfers between devices  22.1 us (15%)
  between operations  13.6 us (9%)
  Pallas kernels  9.26 us (6%)
  local copies, waits for them, and re-layouts  4.1 us (3%)
  other arithmetic  2.73 us (2%)
    all_to_all x5, blocking collectives, exchanged(): return lax.all_to_all(blocks, axis, split_axis=0, concat_axis=0, tiled=True)  68.5 us
    all_to_all x2, waiting for transfers between devices, exchanged(): return lax.all_to_all(blocks, axis, split_axis=0, concat_axis=0, tiled=True)  13.5 us
    all_to_all x2, starting transfers between devices, exchanged(): return lax.all_to_all(blocks, axis, split_axis=0, concat_axis=0, tiled=True)  11.3 us
    ppermute x2, starting transfers between devices, swapped(): return lax.ppermute(x, axis, [(0, 1), (1, 0)])  9.36 us
    all_gather x1, waiting for transfers between devices, body(): lax.all_gather(state_along_y, ('sp_0', 'sp_2'), axis=0, tiled=True)  4.9 us
    pallas_call x1, Pallas kernels, body(): pl.pallas_call(final_kernel, in_specs=[ANY, ANY, ANY] + [VMEM] * 5 + [ANY...  4.41 us
    pallas_call x1, Pallas kernels, body(): pl.pallas_call(state_kernel, in_specs=[SMEM, VMEM, VMEM, ANY, VMEM, VMEM,...  3.56 us
  transfers between devices with their start and end apart: 7, of which 5 were waited for; matrix products, arithmetic and copies ran while one was open for 3% of the time, Pallas kernels for 3%

profile of v5, /device:TPU:1, one launch (start us, length us, event | category | flops | bytes accessed | tf_op | source)
XLA Modules:
  0.0 143.7 jit_solution(17217731745322599415)
XLA Ops:
  6.5 0.8 pad_maximum_fusion.1
  7.3 0.7 broadcast_in_dim.18
  8.0 7.6 %all-to-all-start.1 = ((bf16[8,16,512]{2,1,0:T(8,128)(2,1)}), bf16[8,16,512]{2,1,0:T(8,128)(2,1)S(1)}, u32[]{:S(2)}, u32[]{:S(2)}) async-start(bf16[8,16,512]{2,1,0:T(8,128)(2,1)} %broadcast_in_dim.18), calls=%async_computation.1 | async-start | bytes 262144 | tf_op jit(solution)/shard_map/all_to_all | solution.py:23
  15.6 0.8 pad_maximum_fusion
  16.4 7.2 %all-to-all-done.1 = bf16[8,16,512]{2,1,0:T(8,128)(2,1)S(1)} async-done(((bf16[8,16,512]{2,1,0:T(8,128)(2,1)}), bf16[8,16,512]{2,1,0:T(8,128)(2,1)S(1)}, u32[]{:S(2)}, u32[]{:S(2)}) %all-to-all-start.1) | async-done | bytes 131104 | tf_op jit(solution)/shard_map/all_to_all | solution.py:23
  24.4 12.7 %all_to_all.35 = bf16[8,16,1024]{2,1,0:T(8,128)(2,1)} all-to-all(bf16[8,16,1024]{2,1,0:T(8,128)(2,1)S(1)} %broadcast_in_dim.19), channel_id=1, replica_groups=mesh['sp_0'=8,'sp_1'=8,'sp_2'=2,'tp'=4] {'sp_1'}, dimensions={0} | all-to-all | bytes 524288 | tf_op jit(solution)/shard_map/all_to_all | solution.py:23
  37.1 1.8 %broadcast_in_dim.17 = bf16[4,32,2048]{2,1,0:T(8,128)(2,1)} broadcast(bf16[32,2048]{1,0:T(8,128)(2,1)} %param.16), dimensions={1,2} | broadcast | bytes 655360 | tf_op jit(solution)/shard_map/broadcast_in_dim | solution.py:27
  38.9 3.7 %all-to-all-start = ((bf16[4,32,2048]{2,1,0:T(8,128)(2,1)}), bf16[4,32,2048]{2,1,0:T(8,128)(2,1)S(1)}, u32[]{:S(2)}, u32[]{:S(2)}) async-start(bf16[4,32,2048]{2,1,0:T(8,128)(2,1)} %broadcast_in_dim.17), calls=%async_computation | async-start | bytes 1048576 | tf_op jit(solution)/shard_map/all_to_all | solution.py:23
  42.6 0.7 mul.30
  43.3 6.2 %all-to-all-done = bf16[4,32,2048]{2,1,0:T(8,128)(2,1)S(1)} async-done(((bf16[4,32,2048]{2,1,0:T(8,128)(2,1)}), bf16[4,32,2048]{2,1,0:T(8,128)(2,1)S(1)}, u32[]{:S(2)}, u32[]{:S(2)}) %all-to-all-start) | async-done | bytes 524320 | tf_op jit(solution)/shard_map/all_to_all | solution.py:23
  50.6 7.4 %collective-permute-start = (bf16[128,2048]{1,0:T(8,128)(2,1)S(1)}, bf16[128,2048]{1,0:T(8,128)(2,1)S(1)}, u32[]{:S(2)}, u32[]{:S(2)}) collective-permute-start(bf16[128,2048]{1,0:T(8,128)(2,1)S(1)} %bitcast.24), channel_id=1, source_target_pairs={{0,4},{4,0},{1,5},{5,1},{2,6},{6,2},{3,7},{7,3},{8,12},{12,8},{9,1... | collective-permute-start | bytes 1572872 | tf_op jit(solution)/shard_map/ppermute | solution.py:31
  58.1 1.9 %collective-permute-start.2 = (f32[128,128]{1,0:T(8,128)S(1)}, f32[128,128]{1,0:T(8,128)S(1)}, u32[]{:S(2)}, u32[]{:S(2)}) collective-permute-start(f32[128,128]{1,0:T(8,128)S(1)} %constant_dynamic-slice_fusion), channel_id=1, source_target_pairs={{0,4},{4,0},{1,5},{5,1},{2,6},{6,2},{3,7},{7,3},{8,12},{12,8},{9,1... | collective-permute-start | bytes 196616 | tf_op jit(solution)/shard_map/ppermute | solution.py:31
  60.0 2.2 %collective-permute-start.1 = (bf16[16,2048]{1,0:T(8,128)(2,1)S(1)}, bf16[16,2048]{1,0:T(8,128)(2,1)S(1)}, u32[]{:S(2)}, u32[]{:S(2)}) collective-permute-start(bf16[16,2048]{1,0:T(8,128)(2,1)S(1)} %bitcast.34), channel_id=1, source_target_pairs={{0,4},{4,8},{8,12},{12,16},{16,20},{20,24},{24,28},{28,32},{32,36}... | collective-permute-start | bytes 196616 | tf_op jit(solution)/shard_map/ppermute | solution.py:36
  62.3 1.2 collective-permute-done.1.halo
  63.6 4.9 %all-gather.5.cloned.1.call-done.weights = bf16[2048,512]{1,0:T(8,128)(2,1)} async-done(((bf16[128,512]{1,0:T(8,128)(2,1)}), bf16[2048,512]{1,0:T(8,128)(2,1)}) %all-gather.5.cloned.1.call-update) | async-done | bytes 2097168 | tf_op jit(solution)/shard_map/all_gather | solution.py:294
  68.5 3.6 %chip_state.1 = (bf16[8,144,128]{2,1,0:T(8,128)(2,1)S(1)}, f32[9,128,128]{2,1,0:T(8,128)S(1)}) custom-call(s32[3]{0:T(128)S(1)} %pad_add_fusion.places, bf16[128,2048]{1,0:T(8,128)(2,1)S(1)} %bitcast.25, bf16[128,2048]{1,0:T(8,128)(2,1)S(1)} %collective-permute-done.partner, bf16[2048,512]{1,0:T(8,128)(2,1)} %all-gather.5.cloned.1.call-done.weights, ...), custom_call_target="tpu_custom_call" | custom-call | tf_op jit(solution)/shard_map/chip_state/pallas_call | solution.py:330
  72.0 18.6 %all_to_all.36.arrived = bf16[8,144,128]{2,1,0:T(8,128)(2,1)S(1)} all-to-all(bf16[8,144,128]{2,1,0:T(8,128)(2,1)S(1)} %get-tuple-element.23), channel_id=1, replica_groups=mesh['sp_0'=8,'sp_1'=8,'sp_2'=2,'tp'=4] {'sp_1'}, dimensions={0} | all-to-all | bytes 589824 | tf_op jit(solution)/shard_map/all_to_all | solution.py:23
  90.6 0.7 along_row.1
  91.3 18.4 %all_to_all.37.arrived = bf16[8,144,128]{2,1,0:T(8,128)(2,1)S(1)} all-to-all(bf16[8,144,128]{2,1,0:T(8,128)(2,1)S(1)} %get-tuple-element.24), channel_id=1, replica_groups=mesh['sp_0'=8,'sp_1'=8,'sp_2'=2,'tp'=4] {'sp_0'}, dimensions={0} | all-to-all | bytes 589824 | tf_op jit(solution)/shard_map/all_to_all | solution.py:23
  110.3 5.9 %all_to_all.38.incoming = bf16[2,128,128]{2,1,0:T(8,128)(2,1)S(1)} all-to-all(bf16[2,128,128]{2,1,0:T(8,128)(2,1)S(1)} %enter_chip.1), channel_id=1, replica_groups=mesh['sp_0'=8,'sp_1'=8,'sp_2'=2,'tp'=4] {'sp_2'}, dimensions={0} | all-to-all | bytes 131072 | tf_op jit(solution)/shard_map/all_to_all | solution.py:23
  116.2 2.5 %all-gather.3.cloned.1.call-done.weights = bf16[2048,1024]{1,0:T(8,128)(2,1)} async-done(((bf16[128,1024]{1,0:T(8,128)(2,1)}), bf16[2048,1024]{1,0:T(8,128)(2,1)}) %all-gather.3.cloned.1.call-update) | async-done | bytes 4194320 | tf_op jit(solution)/shard_map/all_gather | solution.py:296
  118.8 4.4 %outputs.1 = bf16[128,2048]{1,0:T(8,128)(2,1)S(1)} custom-call(bf16[16,2048]{1,0:T(8,128)(2,1)} %copy-done.9, bf16[128,2048]{1,0:T(8,128)(2,1)} %bitcast.26, bf16[2048,1024]{1,0:T(8,128)(2,1)} %all-gather.3.cloned.1.call-done.weights, f32[9,128,128]{2,1,0:T(8,128)S(1)} %get-tuple-element.22.carried, f32[3,256]{1,0:T(4,128)S(1)} %copy-done.3, ...), custom_call_target="tpu_custom_call" | custom-call | tf_op jit(solution)/shard_map/outputs/pallas_call | solution.py:373
  123.2 12.9 %all_to_all.39 = bf16[4,32,2048]{2,1,0:T(8,128)(2,1)S(1)} all-to-all(bf16[4,32,2048]{2,1,0:T(8,128)(2,1)S(1)} %bitcast.27), channel_id=1, replica_groups=mesh['sp_0'=8,'sp_1'=8,'sp_2'=2,'tp'=4] {'tp'}, dimensions={0} | all-to-all | bytes 1048576 | tf_op jit(solution)/shard_map/all_to_all | solution.py:23
  136.1 0.7 reduce_sum.22
  (39 shorter events, 2.5 us)
Async XLA Ops:
  6.5 43.6 %copy-start.7 = (bf16[256,256,1]{1,0,2:T(8,128)(2,1)S(1)}, bf16[256,256,1]{1,0,2:T(8,128)(2,1)}, u32[]{:S(2)}) copy-start(bf16[256,256,1]{1,0,2:T(8,128)(2,1)} %constant.43) | copy-start | bytes 393220
  8.0 15.7 %all-to-all-start.1 = ((bf16[8,16,512]{2,1,0:T(8,128)(2,1)}), bf16[8,16,512]{2,1,0:T(8,128)(2,1)S(1)}, u32[]{:S(2)}, u32[]{:S(2)}) async-start(bf16[8,16,512]{2,1,0:T(8,128)(2,1)} %broadcast_in_dim.18), calls=%async_computation.1 | async-start | bytes 262144 | tf_op jit(solution)/shard_map/all_to_all | solution.py:23
  15.6 52.9 %all-gather.5.cloned.1.call-start = ((), (), s32[]{:S(2)}) async-start(), calls=%async_computation.8 | async-start | bytes 2228224 | tf_op jit(solution)/shard_map/all_gather | solution.py:294
  23.6 0.7 copy-start.6
  24.3 94.5 %all-gather.3.cloned.1.call-start = ((), (), s32[]{:S(2)}) async-start(), calls=%async_computation.7 | async-start | bytes 4456448 | tf_op jit(solution)/shard_map/all_gather | solution.py:296
  24.4 33.6 %copy-start.2 = (f32[128,256]{1,0:T(8,128)S(1)}, f32[128,256]{1,0:T(8,128)}, u32[]{:S(2)}) copy-start(f32[128,256]{1,0:T(8,128)} %fade.1) | copy-start | bytes 393220
  37.1 31.4 %copy-start.4 = (f32[256]{0:T(256)S(1)}, f32[256]{0:T(256)}, u32[]{:S(2)}) copy-start(f32[256]{0:T(256)} %param.25) | copy-start | bytes 3076
  38.9 10.6 %all-to-all-start = ((bf16[4,32,2048]{2,1,0:T(8,128)(2,1)}), bf16[4,32,2048]{2,1,0:T(8,128)(2,1)S(1)}, u32[]{:S(2)}, u32[]{:S(2)}) async-start(bf16[4,32,2048]{2,1,0:T(8,128)(2,1)} %broadcast_in_dim.17), calls=%async_computation | async-start | bytes 1048576 | tf_op jit(solution)/shard_map/all_to_all | solution.py:23
  50.5 68.3 %copy-start.1 = (bf16[256,2048]{1,0:T(8,128)(2,1)S(1)}, bf16[256,2048]{1,0:T(8,128)(2,1)}, u32[]{:S(2)}) copy-start(bf16[256,2048]{1,0:T(8,128)(2,1)} %w_filter.1) | copy-start | bytes 3145732
  50.5 68.3 %copy-start.3 = (f32[3,256]{1,0:T(4,128)S(1)}, f32[3,256]{1,0:T(4,128)}, u32[]{:S(2)}) copy-start(f32[3,256]{1,0:T(4,128)} %taps.1) | copy-start | bytes 9220
  50.5 68.3 %copy-start.5 = (f32[128]{0:T(128)S(1)}, f32[128]{0:T(128)}, u32[]{:S(2)}) copy-start(f32[128]{0:T(128)} %param.27) | copy-start | bytes 1540
  50.6 68.2 %copy-start = (bf16[8,16,8,256]{3,2,0,1:T(8,128)(2,1)}, bf16[8,16,8,256]{3,2,0,1:T(8,128)(2,1)S(1)}, u32[]{:S(2)}) copy-start(bf16[8,16,8,256]{3,2,0,1:T(8,128)(2,1)S(1)} %copy.22) | copy-start | bytes 1572868
  50.6 13.0 %collective-permute-start = (bf16[128,2048]{1,0:T(8,128)(2,1)S(1)}, bf16[128,2048]{1,0:T(8,128)(2,1)S(1)}, u32[]{:S(2)}, u32[]{:S(2)}) collective-permute-start(bf16[128,2048]{1,0:T(8,128)(2,1)S(1)} %bitcast.24), channel_id=1, source_target_pairs={{0,4},{4,0},{1,5},{5,1},{2,6},{6,2},{3,7},{7,3},{8,12},{12,8},{9,1... | collective-permute-start | bytes 1572872 | tf_op jit(solution)/shard_map/ppermute | solution.py:31
  58.1 4.3 %collective-permute-start.2 = (f32[128,128]{1,0:T(8,128)S(1)}, f32[128,128]{1,0:T(8,128)S(1)}, u32[]{:S(2)}, u32[]{:S(2)}) collective-permute-start(f32[128,128]{1,0:T(8,128)S(1)} %constant_dynamic-slice_fusion), channel_id=1, source_target_pairs={{0,4},{4,0},{1,5},{5,1},{2,6},{6,2},{3,7},{7,3},{8,12},{12,8},{9,1... | collective-permute-start | bytes 196616 | tf_op jit(solution)/shard_map/ppermute | solution.py:31
  60.0 3.6 %collective-permute-start.1 = (bf16[16,2048]{1,0:T(8,128)(2,1)S(1)}, bf16[16,2048]{1,0:T(8,128)(2,1)S(1)}, u32[]{:S(2)}, u32[]{:S(2)}) collective-permute-start(bf16[16,2048]{1,0:T(8,128)(2,1)S(1)} %bitcast.34), channel_id=1, source_target_pairs={{0,4},{4,8},{8,12},{12,16},{16,20},{20,24},{24,28},{28,32},{32,36}... | collective-permute-start | bytes 196616 | tf_op jit(solution)/shard_map/ppermute | solution.py:36
  62.3 6.1 %copy-start.8 = (f32[128,128]{1,0:T(8,128)}, f32[128,128]{1,0:T(8,128)S(1)}, u32[]{:S(2)}) copy-start(f32[128,128]{1,0:T(8,128)S(1)} %collective-permute-done.2.partner_fade) | copy-start | bytes 196612
  63.6 55.2 %copy-start.9 = (bf16[16,2048]{1,0:T(8,128)(2,1)}, bf16[16,2048]{1,0:T(8,128)(2,1)S(1)}, u32[]{:S(2)}) copy-start(bf16[16,2048]{1,0:T(8,128)(2,1)S(1)} %collective-permute-done.1.halo) | copy-start | bytes 196612
Sparse Core Ops, SparseCore 0:
  24.4 44.0 all-gather.4
  70.6 48.1 all-gather.2

commit v6 on v4

--- a/solution.py
+++ b/solution.py
@@ -290,7 +290,12 @@
     state_rows = jnp.concatenate([retention_gate_matrix, w_input], axis=1)
     state_along_y = sent_to_all(state_rows, "sp_1").reshape(-1, state_rows.shape[1])
     rest_rows = jnp.concatenate([w_query, w_filter_b, w_filter_c, w_filter_v], axis=1)
-    state_along_y, rest_rows = lax.optimization_barrier((state_along_y, rest_rows))
+    fade = additive_fade_log
+    head = lambda a, k: lax.dynamic_slice_in_dim(a, k * HEAD_DIM, HEAD_DIM, axis=1)
+    partner_fade = swapped(head(fade, 1 - c), "sp_2")
+    state_along_y, rest_rows, partner_fade = lax.optimization_barrier(
+        (state_along_y, rest_rows, partner_fade)
+    )
     state_weights = lax.all_gather(state_along_y, ("sp_0", "sp_2"), axis=0, tiled=True)
     rest_along_y = sent_to_all(rest_rows, "sp_1").reshape(-1, rest_rows.shape[1])
     rest_weights = lax.all_gather(rest_along_y, ("sp_0", "sp_2"), axis=0, tiled=True)
@@ -314,10 +319,6 @@
     ).astype(bf16).reshape(length, width)
     partner = swapped(own, "sp_2")
     halo = shifted(own[length - HALO :], SP)
-
-    fade = additive_fade_log
-    head = lambda a, k: lax.dynamic_slice_in_dim(a, k * HEAD_DIM, HEAD_DIM, axis=1)
-    partner_fade = swapped(head(fade, 1 - c), "sp_2")
 
     places = jnp.stack([z, y, c])
     partner, halo, partner_fade, places = lax.optimization_barrier(

time: 144 us -> 144 us (level)
  waiting for transfers between devices: 22.4 us -> 18.7 us
  blocking collectives: 68.4 us -> 70.6 us
    all_to_all x2, waiting for transfers between devices: 13.5 us -> 8.01 us  [exchanged(): return lax.all_to_all(blocks, axis, split_axis=0, concat_axis=0, tiled=True)]
    all_to_all x5, blocking collectives: 68.4 us -> 70.6 us  [exchanged(): return lax.all_to_all(blocks, axis, split_axis=0, concat_axis=0, tiled=True)]
    all_gather x1, waiting for transfers between devices: 4.9 us -> 6.68 us  [body(): lax.all_gather(state_along_y, ('sp_0', 'sp_2'), axis=0, tiled=True)]
  transfers between devices with their start and end apart: 7 -> 7, of which waited for: 5 -> 6; matrix products, arithmetic and copies ran while one was open for 3% -> 4% of each run, Pallas kernels for 3% -> 3%
where the time goes in v6:
time: 144 us
  blocking collectives  70.6 us (49%)
  starting transfers between devices  23.9 us (17%)
  waiting for transfers between devices  18.7 us (13%)
  between operations  13.6 us (9%)
  Pallas kernels  8.84 us (6%)
  local copies, waits for them, and re-layouts  4.98 us (3%)
  other arithmetic  2.74 us (2%)
    all_to_all x5, blocking collectives, exchanged(): return lax.all_to_all(blocks, axis, split_axis=0, concat_axis=0, tiled=True)  70.6 us
    all_to_all x2, starting transfers between devices, exchanged(): return lax.all_to_all(blocks, axis, split_axis=0, concat_axis=0, tiled=True)  11.1 us
    ppermute x2, starting transfers between devices, swapped(): return lax.ppermute(x, axis, [(0, 1), (1, 0)])  10.6 us
    all_to_all x2, waiting for transfers between devices, exchanged(): return lax.all_to_all(blocks, axis, split_axis=0, concat_axis=0, tiled=True)  8.01 us
    all_gather x1, waiting for transfers between devices, body(): lax.all_gather(state_along_y, ('sp_0', 'sp_2'), axis=0, tiled=True)  6.68 us
    pallas_call x1, Pallas kernels, body(): pl.pallas_call(final_kernel, in_specs=[ANY, ANY, ANY] + [VMEM] * 5 + [ANY...  4.23 us
    pallas_call x1, Pallas kernels, body(): pl.pallas_call(state_kernel, in_specs=[SMEM, VMEM, VMEM, ANY, VMEM, VMEM,...  3.32 us
  transfers between devices with their start and end apart: 7, of which 6 were waited for; matrix products, arithmetic and copies ran while one was open for 4% of the time, Pallas kernels for 3%

profile of v6, /device:TPU:1, one launch (start us, length us, event | category | flops | bytes accessed | tf_op | source)
XLA Modules:
  0.0 143.7 jit_solution(9958308648631653282)
XLA Ops:
  6.5 0.8 pad_maximum_fusion.1
  8.0 7.6 %all-to-all-start.1 = ((bf16[8,16,512]{2,1,0:T(8,128)(2,1)}), bf16[8,16,512]{2,1,0:T(8,128)(2,1)S(1)}, u32[]{:S(2)}, u32[]{:S(2)}) async-start(bf16[8,16,512]{2,1,0:T(8,128)(2,1)} %broadcast_in_dim.18), calls=%async_computation.1 | async-start | bytes 262144 | tf_op jit(solution)/shard_map/all_to_all | solution.py:23
  15.6 0.8 constant_dynamic-slice_fusion
  16.5 4.5 %collective-permute-start.2 = (f32[128,128]{1,0:T(8,128)S(1)}, f32[128,128]{1,0:T(8,128)S(1)}, u32[]{:S(2)}, u32[]{:S(2)}) collective-permute-start(f32[128,128]{1,0:T(8,128)S(1)} %constant_dynamic-slice_fusion), channel_id=1, source_target_pairs={{0,4},{4,0},{1,5},{5,1},{2,6},{6,2},{3,7},{7,3},{8,12},{12,8},{9,1... | collective-permute-start | bytes 196616 | tf_op jit(solution)/shard_map/ppermute | solution.py:31
  21.0 0.8 pad_maximum_fusion
  21.9 1.8 %all-to-all-done.1 = bf16[8,16,512]{2,1,0:T(8,128)(2,1)S(1)} async-done(((bf16[8,16,512]{2,1,0:T(8,128)(2,1)}), bf16[8,16,512]{2,1,0:T(8,128)(2,1)S(1)}, u32[]{:S(2)}, u32[]{:S(2)}) %all-to-all-start.1) | async-done | bytes 131104 | tf_op jit(solution)/shard_map/all_to_all | solution.py:23
  24.4 14.8 %all_to_all.35 = bf16[8,16,1024]{2,1,0:T(8,128)(2,1)} all-to-all(bf16[8,16,1024]{2,1,0:T(8,128)(2,1)S(1)} %broadcast_in_dim.19), channel_id=1, replica_groups=mesh['sp_0'=8,'sp_1'=8,'sp_2'=2,'tp'=4] {'sp_1'}, dimensions={0} | all-to-all | bytes 524288 | tf_op jit(solution)/shard_map/all_to_all | solution.py:23
  39.2 1.8 %broadcast_in_dim.17 = bf16[4,32,2048]{2,1,0:T(8,128)(2,1)} broadcast(bf16[32,2048]{1,0:T(8,128)(2,1)} %param.16), dimensions={1,2} | broadcast | bytes 655360 | tf_op jit(solution)/shard_map/broadcast_in_dim | solution.py:27
  41.0 3.5 %all-to-all-start = ((bf16[4,32,2048]{2,1,0:T(8,128)(2,1)}), bf16[4,32,2048]{2,1,0:T(8,128)(2,1)S(1)}, u32[]{:S(2)}, u32[]{:S(2)}) async-start(bf16[4,32,2048]{2,1,0:T(8,128)(2,1)} %broadcast_in_dim.17), calls=%async_computation | async-start | bytes 1048576 | tf_op jit(solution)/shard_map/all_to_all | solution.py:23
  44.5 0.7 mul.30
  45.2 6.3 %all-to-all-done = bf16[4,32,2048]{2,1,0:T(8,128)(2,1)S(1)} async-done(((bf16[4,32,2048]{2,1,0:T(8,128)(2,1)}), bf16[4,32,2048]{2,1,0:T(8,128)(2,1)S(1)}, u32[]{:S(2)}, u32[]{:S(2)}) %all-to-all-start) | async-done | bytes 524320 | tf_op jit(solution)/shard_map/all_to_all | solution.py:23
  52.5 6.1 %collective-permute-start = (bf16[128,2048]{1,0:T(8,128)(2,1)S(1)}, bf16[128,2048]{1,0:T(8,128)(2,1)S(1)}, u32[]{:S(2)}, u32[]{:S(2)}) collective-permute-start(bf16[128,2048]{1,0:T(8,128)(2,1)S(1)} %bitcast.24), channel_id=1, source_target_pairs={{0,4},{4,0},{1,5},{5,1},{2,6},{6,2},{3,7},{7,3},{8,12},{12,8},{9,1... | collective-permute-start | bytes 1572872 | tf_op jit(solution)/shard_map/ppermute | solution.py:31
  58.7 2.1 %collective-permute-start.1 = (bf16[16,2048]{1,0:T(8,128)(2,1)S(1)}, bf16[16,2048]{1,0:T(8,128)(2,1)S(1)}, u32[]{:S(2)}, u32[]{:S(2)}) collective-permute-start(bf16[16,2048]{1,0:T(8,128)(2,1)S(1)} %bitcast.34), channel_id=1, source_target_pairs={{0,4},{4,8},{8,12},{12,16},{16,20},{20,24},{24,28},{28,32},{32,36}... | collective-permute-start | bytes 196616 | tf_op jit(solution)/shard_map/ppermute | solution.py:36
  60.8 1.2 collective-permute-done.1.halo
  62.1 6.7 %all-gather.5.cloned.1.call-done.weights = bf16[2048,512]{1,0:T(8,128)(2,1)} async-done(((bf16[128,512]{1,0:T(8,128)(2,1)}), bf16[2048,512]{1,0:T(8,128)(2,1)}) %all-gather.5.cloned.1.call-update) | async-done | bytes 2097168 | tf_op jit(solution)/shard_map/all_gather | solution.py:299
  68.8 3.3 %chip_state.1 = (bf16[8,144,128]{2,1,0:T(8,128)(2,1)S(1)}, f32[9,128,128]{2,1,0:T(8,128)S(1)}) custom-call(s32[3]{0:T(128)S(1)} %pad_add_fusion.places, bf16[128,2048]{1,0:T(8,128)(2,1)S(1)} %bitcast.25, bf16[128,2048]{1,0:T(8,128)(2,1)S(1)} %collective-permute-done.partner, bf16[2048,512]{1,0:T(8,128)(2,1)} %all-gather.5.cloned.1.call-done.weights, ...), custom_call_target="tpu_custom_call" | custom-call | tf_op jit(solution)/shard_map/chip_state/pallas_call | solution.py:331
  72.1 18.6 %all_to_all.36.arrived = bf16[8,144,128]{2,1,0:T(8,128)(2,1)S(1)} all-to-all(bf16[8,144,128]{2,1,0:T(8,128)(2,1)S(1)} %get-tuple-element.25), channel_id=1, replica_groups=mesh['sp_0'=8,'sp_1'=8,'sp_2'=2,'tp'=4] {'sp_1'}, dimensions={0} | all-to-all | bytes 589824 | tf_op jit(solution)/shard_map/all_to_all | solution.py:23
  90.7 0.7 along_row.1
  91.4 18.7 %all_to_all.37.arrived = bf16[8,144,128]{2,1,0:T(8,128)(2,1)S(1)} all-to-all(bf16[8,144,128]{2,1,0:T(8,128)(2,1)S(1)} %get-tuple-element.26), channel_id=1, replica_groups=mesh['sp_0'=8,'sp_1'=8,'sp_2'=2,'tp'=4] {'sp_0'}, dimensions={0} | all-to-all | bytes 589824 | tf_op jit(solution)/shard_map/all_to_all | solution.py:23
  110.7 5.7 %all_to_all.38.incoming = bf16[2,128,128]{2,1,0:T(8,128)(2,1)S(1)} all-to-all(bf16[2,128,128]{2,1,0:T(8,128)(2,1)S(1)} %enter_chip.1), channel_id=1, replica_groups=mesh['sp_0'=8,'sp_1'=8,'sp_2'=2,'tp'=4] {'sp_2'}, dimensions={0} | all-to-all | bytes 131072 | tf_op jit(solution)/shard_map/all_to_all | solution.py:23
  116.4 2.6 %all-gather.3.cloned.1.call-done.weights = bf16[2048,1024]{1,0:T(8,128)(2,1)} async-done(((bf16[128,1024]{1,0:T(8,128)(2,1)}), bf16[2048,1024]{1,0:T(8,128)(2,1)}) %all-gather.3.cloned.1.call-update) | async-done | bytes 4194320 | tf_op jit(solution)/shard_map/all_gather | solution.py:301
  119.1 4.2 %outputs.1 = bf16[128,2048]{1,0:T(8,128)(2,1)S(1)} custom-call(bf16[16,2048]{1,0:T(8,128)(2,1)} %copy-done.9, bf16[128,2048]{1,0:T(8,128)(2,1)} %bitcast.26, bf16[2048,1024]{1,0:T(8,128)(2,1)} %all-gather.3.cloned.1.call-done.weights, f32[9,128,128]{2,1,0:T(8,128)S(1)} %get-tuple-element.24.carried, f32[3,256]{1,0:T(4,128)S(1)} %copy-done.3, ...), custom_call_target="tpu_custom_call" | custom-call | tf_op jit(solution)/shard_map/outputs/pallas_call | solution.py:374
  123.3 12.8 %all_to_all.39 = bf16[4,32,2048]{2,1,0:T(8,128)(2,1)S(1)} all-to-all(bf16[4,32,2048]{2,1,0:T(8,128)(2,1)S(1)} %bitcast.27), channel_id=1, replica_groups=mesh['sp_0'=8,'sp_1'=8,'sp_2'=2,'tp'=4] {'tp'}, dimensions={0} | all-to-all | bytes 1048576 | tf_op jit(solution)/shard_map/all_to_all | solution.py:23
  136.1 0.7 reduce_sum.22
  (39 shorter events, 3.3 us)
Async XLA Ops:
  6.5 45.5 %copy-start.7 = (bf16[256,256,1]{1,0,2:T(8,128)(2,1)S(1)}, bf16[256,256,1]{1,0,2:T(8,128)(2,1)}, u32[]{:S(2)}) copy-start(bf16[256,256,1]{1,0,2:T(8,128)(2,1)} %constant.43) | copy-start | bytes 393220
  8.0 15.7 %all-to-all-start.1 = ((bf16[8,16,512]{2,1,0:T(8,128)(2,1)}), bf16[8,16,512]{2,1,0:T(8,128)(2,1)S(1)}, u32[]{:S(2)}, u32[]{:S(2)}) async-start(bf16[8,16,512]{2,1,0:T(8,128)(2,1)} %broadcast_in_dim.18), calls=%async_computation.1 | async-start | bytes 262144 | tf_op jit(solution)/shard_map/all_to_all | solution.py:23
  15.6 53.2 %all-gather.5.cloned.1.call-start = ((), (), s32[]{:S(2)}) async-start(), calls=%async_computation.8 | async-start | bytes 2228224 | tf_op jit(solution)/shard_map/all_gather | solution.py:299
  16.5 5.4 %collective-permute-start.2 = (f32[128,128]{1,0:T(8,128)S(1)}, f32[128,128]{1,0:T(8,128)S(1)}, u32[]{:S(2)}, u32[]{:S(2)}) collective-permute-start(f32[128,128]{1,0:T(8,128)S(1)} %constant_dynamic-slice_fusion), channel_id=1, source_target_pairs={{0,4},{4,0},{1,5},{5,1},{2,6},{6,2},{3,7},{7,3},{8,12},{12,8},{9,1... | collective-permute-start | bytes 196616 | tf_op jit(solution)/shard_map/ppermute | solution.py:31
  21.9 46.9 %copy-start.8 = (f32[128,128]{1,0:T(8,128)}, f32[128,128]{1,0:T(8,128)S(1)}, u32[]{:S(2)}) copy-start(f32[128,128]{1,0:T(8,128)S(1)} %collective-permute-done.2.partner_fade) | copy-start | bytes 196612
  23.6 0.7 copy-start.6
  24.3 94.8 %all-gather.3.cloned.1.call-start = ((), (), s32[]{:S(2)}) async-start(), calls=%async_computation.7 | async-start | bytes 4456448 | tf_op jit(solution)/shard_map/all_gather | solution.py:301
  39.2 29.6 %copy-start.2 = (f32[128,256]{1,0:T(8,128)S(1)}, f32[128,256]{1,0:T(8,128)}, u32[]{:S(2)}) copy-start(f32[128,256]{1,0:T(8,128)} %fade.1) | copy-start | bytes 393220
  39.2 29.6 %copy-start.4 = (f32[256]{0:T(256)S(1)}, f32[256]{0:T(256)}, u32[]{:S(2)}) copy-start(f32[256]{0:T(256)} %param.25) | copy-start | bytes 3076
  41.0 10.4 %all-to-all-start = ((bf16[4,32,2048]{2,1,0:T(8,128)(2,1)}), bf16[4,32,2048]{2,1,0:T(8,128)(2,1)S(1)}, u32[]{:S(2)}, u32[]{:S(2)}) async-start(bf16[4,32,2048]{2,1,0:T(8,128)(2,1)} %broadcast_in_dim.17), calls=%async_computation | async-start | bytes 1048576 | tf_op jit(solution)/shard_map/all_to_all | solution.py:23
  52.4 66.7 %copy-start.1 = (bf16[256,2048]{1,0:T(8,128)(2,1)S(1)}, bf16[256,2048]{1,0:T(8,128)(2,1)}, u32[]{:S(2)}) copy-start(bf16[256,2048]{1,0:T(8,128)(2,1)} %w_filter.1) | copy-start | bytes 3145732
  52.4 66.7 %copy-start.3 = (f32[3,256]{1,0:T(4,128)S(1)}, f32[3,256]{1,0:T(4,128)}, u32[]{:S(2)}) copy-start(f32[3,256]{1,0:T(4,128)} %taps.1) | copy-start | bytes 9220
  52.4 66.6 %copy-start.5 = (f32[128]{0:T(128)S(1)}, f32[128]{0:T(128)}, u32[]{:S(2)}) copy-start(f32[128]{0:T(128)} %param.27) | copy-start | bytes 1540
  52.5 66.6 %copy-start = (bf16[8,16,8,256]{3,2,0,1:T(8,128)(2,1)}, bf16[8,16,8,256]{3,2,0,1:T(8,128)(2,1)S(1)}, u32[]{:S(2)}) copy-start(bf16[8,16,8,256]{3,2,0,1:T(8,128)(2,1)S(1)} %copy.22) | copy-start | bytes 1572868
  52.5 9.6 %collective-permute-start = (bf16[128,2048]{1,0:T(8,128)(2,1)S(1)}, bf16[128,2048]{1,0:T(8,128)(2,1)S(1)}, u32[]{:S(2)}, u32[]{:S(2)}) collective-permute-start(bf16[128,2048]{1,0:T(8,128)(2,1)S(1)} %bitcast.24), channel_id=1, source_target_pairs={{0,4},{4,0},{1,5},{5,1},{2,6},{6,2},{3,7},{7,3},{8,12},{12,8},{9,1... | collective-permute-start | bytes 1572872 | tf_op jit(solution)/shard_map/ppermute | solution.py:31
  58.7 3.4 %collective-permute-start.1 = (bf16[16,2048]{1,0:T(8,128)(2,1)S(1)}, bf16[16,2048]{1,0:T(8,128)(2,1)S(1)}, u32[]{:S(2)}, u32[]{:S(2)}) collective-permute-start(bf16[16,2048]{1,0:T(8,128)(2,1)S(1)} %bitcast.34), channel_id=1, source_target_pairs={{0,4},{4,8},{8,12},{12,16},{16,20},{20,24},{24,28},{28,32},{32,36}... | collective-permute-start | bytes 196616 | tf_op jit(solution)/shard_map/ppermute | solution.py:36
  62.1 57.0 %copy-start.9 = (bf16[16,2048]{1,0:T(8,128)(2,1)}, bf16[16,2048]{1,0:T(8,128)(2,1)S(1)}, u32[]{:S(2)}) copy-start(bf16[16,2048]{1,0:T(8,128)(2,1)S(1)} %collective-permute-done.1.halo) | copy-start | bytes 196612
Sparse Core Ops, SparseCore 0:
  24.4 44.2 all-gather.4
  70.9 48.1 all-gather.2
